TPU v7x, 32 devices: a whole 2x2x4 slice. The times are simulated.
32 devices in a mesh: sp: 8 (over z, core), tp: 4 (over y, x).
Axes of the slice: x: 2, y: 2, z: 4, core: 2. Of those that a mesh axis runs over, the one named last changes fastest.
Arguments:
- stream: bfloat16 [2048, 1024], P('tp', 'sp')
- values_in: bfloat16 [1024, 1024], P('tp', 'sp'), may hold values from -6 to 6
- in_gate: bfloat16 [1024, 1024], P('tp', 'sp'), may hold values from -6 to 6
- out_gate: bfloat16 [1024, 1024], P('tp', 'sp'), may hold values from -6 to 6
- documents: int32 [1024], P('sp'), may hold values from 0 to 15, never falling along the last dimension, each value on 1 to 256 neighbouring positions
- conv_taps: float32 [3, 1024], P(None, 'tp'), may hold values from -3.5 to 3.5
- head_gain: float32 [1024], P('tp'), may hold values from 0.1 to 1.9
- mix_weight: bfloat16 [1024, 2048], P('tp'), may hold values from -0.25 to 0.25
- norm_gain: float32 [2048], P('tp'), may hold values from 0.1 to 1.9
- routes: int32 [1024, 4], P('sp'), may hold values from 0 to 7, all different within a row; in each aligned block of 128 rows (0 to 127, 128 to 255, ...) at most 96 rows name the same one
- route_weight: float32 [1024, 4], P('sp'), may hold values from 0.2 to 1
- expert_gate: bfloat16 [8, 2048, 2048], P('sp', None, 'tp'), may hold values from -0.125 to 0.125
- expert_up: bfloat16 [8, 2048, 2048], P('sp', None, 'tp'), may hold values from -0.125 to 0.125
- expert_down: bfloat16 [8, 2048, 2048], P('sp', None, 'tp'), may hold values from -0.125 to 0.125
- shared_gate: bfloat16 [2048, 2048], P(None, 'tp'), may hold values from -0.125 to 0.125
- shared_up: bfloat16 [2048, 2048], P(None, 'tp'), may hold values from -0.125 to 0.125
- shared_down: bfloat16 [2048, 2048], P('tp'), may hold values from -0.1875 to 0.1875
Outputs:
- layer_out: bfloat16 [2048, 1024], P('tp', 'sp')
Inputs may be any that keep to these rules, and one draw needn't show every extreme that they name: `routes`: each row names 4 different experts. In each aligned block of 128 rows no expert is named by more than 96 rows, a bound that some block reaches. `documents`: document numbers never fall along the positions; each document has 1 to 256 positions, and one has exactly that many.
All inputs are finite; a program needn't handle non-finite values.
Results may differ from a plain program's by a relative error of at most 0.015.
Values may be sent and summed in bfloat16 or wider, within the bound.
A program may use at most 64 MiB of HBM per device.

v0:
```python
import functools

import jax
import jax.numpy as jnp
from jax import lax
from jax.experimental import pallas as pl
from jax.experimental.pallas import tpu as pltpu
from jax.sharding import PartitionSpec as P

HEAD = 64
CORES = 2
CHUNKS = 8
SUB = 8
PLAN = (1, 1, 1, 5, 0)
ALONG_Z = (1, 2)
epsilon = 1e-06
MESH = pl.DeviceIdType.MESH
F32 = jnp.float32
BF16 = jnp.bfloat16


def flipped(index, mask):
    bit = 1
    out = index
    while bit <= mask:
        if mask & bit:
            out = out + bit - 2 * bit * lax.rem(lax.div(index, bit), 2)
        bit *= 2
    return out


def dot(left, right):
    return jnp.dot(left, right, preferred_element_type=F32)


def silu(value):
    return value / (1.0 + jnp.exp(-value))


def column_of(row, width):
    return jnp.broadcast_to(row, (width, row.shape[1])).T


def kernel(
    n_sp, n_tp,
    stream, values_in, in_gate, out_gate, documents, conv_taps, head_gain, mix_weight,
    norm_gain, routes, route_weight, expert_gate, expert_up, expert_down,
    shared_gate, shared_up, shared_down,
    out,
    mix_w, gate_w, up_w, sgate_w, sup_w, sdown_w, down_w,
    tail_s, prev_r, prev_docs, mix_s, mix_r, hidden_v, x_all, ss_s, ss_r, meta_r,
    mid_v, shared_v, acc_v, pr_s, pr_r, rs_s, rs_r, rd_r, rz_r, zr_s, zr_r,
    load_sem, local_sem, halo_send, halo_recv, mix_send, mix_recv, ss_send, ss_recv,
    meta_send, meta_recv, x_recv, xs_tp, xs_z, xs_d, xs_n, xs_p, wd_send, wd_recv,
    pr_send, pr_recv, rs_send, rs_recv, zr_send, zr_recv, rz_send, rz_recv,
):
    sp = lax.axis_index("sp")
    tp = lax.axis_index("tp")
    z = lax.div(sp, CORES)
    core = lax.rem(sp, CORES)
    n_z = n_sp // CORES
    feats, pos = stream.shape
    chans = values_in.shape[0]
    width = feats * n_tp
    hid = gate_w.shape[1]
    partner = {"sp": z * CORES + 1 - core}
    peers = [flipped(tp, d) for d in range(1, n_tp)]
    square = n_tp == 4 and n_z > 1
    near = peers[:2] if square else peers
    along_z = [d for d in ALONG_Z if d < n_z] if square else []
    layers = [flipped(z, d) for d in range(n_z)]
    pending = []

    def send(src, dst, ssem, rsem, device):
        copy = pltpu.make_async_remote_copy(
            src_ref=src, dst_ref=dst, send_sem=ssem, recv_sem=rsem,
            device_id=device, device_id_type=MESH,
        )
        copy.start()
        pending.append(copy)

    def arrived(dst, rsem):
        pltpu.make_async_remote_copy(
            src_ref=dst, dst_ref=dst, send_sem=rsem, recv_sem=rsem,
            device_id=partner, device_id_type=MESH,
        ).wait_recv()

    loads = [
        pltpu.make_async_copy(src, dst, load_sem.at[i])
        for i, (src, dst) in enumerate([
            (mix_weight, mix_w), (shared_gate, sgate_w), (shared_up, sup_w),
            (shared_down, sdown_w), (expert_gate.at[0], gate_w), (expert_up.at[0], up_w),
        ])
    ]
    loads[0].start()

    barrier = pltpu.get_barrier_semaphore()
    for peer in peers:
        pl.semaphore_signal(barrier, inc=1, device_id={"tp": peer}, device_id_type=MESH)
    for d in range(1, n_sp):
        pl.semaphore_signal(
            barrier, inc=1, device_id={"sp": lax.rem(sp + d, n_sp)}, device_id_type=MESH
        )
    pl.semaphore_wait(barrier, n_tp - 1 + n_sp - 1)

    product = values_in[...].astype(F32) * in_gate[...].astype(F32)
    tail_s[...] = product.T[pos - SUB:, :]
    after = {"sp": lax.rem(sp + 1, n_sp)}
    send(tail_s, prev_r.at[pl.ds(pos - SUB, SUB)], halo_send.at[0], halo_recv.at[0], after)
    send(documents, prev_docs, halo_send.at[1], halo_recv.at[1], after)

    rows = hid // CHUNKS

    sent_chunks = []

    def send_chunks(stage):
        for _ in range(PLAN[stage]):
            send_down(len(sent_chunks))
            sent_chunks.append(stage)

    def send_down(chunk):
        for d, peer in enumerate(peers):
            start = pl.multiple_of(peer * hid + chunk * rows, rows)
            send(
                expert_down.at[0, pl.ds(start, rows), :],
                down_w.at[tp, pl.ds(chunk * rows, rows), :],
                wd_send.at[d, chunk], wd_recv.at[tp, chunk], {"tp": peer},
            )

    send_chunks(0)
    own_down = pltpu.make_async_copy(
        expert_down.at[0, pl.ds(pl.multiple_of(tp * hid, hid), hid), :], down_w.at[tp], local_sem
    )
    for load in loads[1:]:
        load.start()
    own_down.start()

    named = routes[...]
    weights = route_weight[...]
    meta_rows = meta_r.shape[1]
    at_row = lax.broadcasted_iota(jnp.int32, (meta_rows, pos), 0)
    table = jnp.zeros((meta_rows, pos), F32)
    for k in range(routes.shape[0]):
        table = table + jnp.where(at_row == named[k:k + 1, :], weights[k:k + 1, :], 0.0)
    taps = [column_of(conv_taps[j:j + 1, :], pos) for j in range(3)]
    stream_t = stream[...].astype(F32).T

    prev_r[: pos - SUB, :] = jnp.zeros((pos - SUB, chans), F32)
    arrived(prev_r.at[pl.ds(pos - SUB, SUB)], halo_recv.at[0])
    arrived(prev_docs, halo_recv.at[1])
    before = prev_r[...].T
    docs = documents[...]
    docs_before = jnp.where(sp > 0, prev_docs[...], -1)
    lane_c = lax.broadcasted_iota(jnp.int32, (chans, pos), 1)
    lane_1 = lax.broadcasted_iota(jnp.int32, (1, pos), 1)
    convolved = taps[2] * product
    for shift in (1, 2):
        moved = jnp.where(lane_c < shift, pltpu.roll(before, shift, 1), pltpu.roll(product, shift, 1))
        ids = jnp.where(lane_1 < shift, pltpu.roll(docs_before, shift, 1), pltpu.roll(docs, shift, 1))
        convolved = convolved + jnp.where(ids == docs, taps[2 - shift] * moved, 0.0)
    mixed = out_gate[...].astype(F32) * convolved
    heads = mixed.reshape(chans // HEAD, HEAD, pos)
    heads = heads * lax.rsqrt(jnp.mean(heads * heads, axis=1, keepdims=True) + epsilon)
    heads_t = (heads.reshape(chans, pos).T * head_gain[...]).astype(BF16)

    loads[0].wait()
    for b, peer in enumerate(peers + [tp]):
        cols = pl.ds(pl.multiple_of(peer * feats, feats), feats)
        mix_s[b] = dot(heads_t, mix_w[:, cols]).astype(BF16)
        if b < n_tp - 1:
            send(mix_s.at[b], mix_r.at[b], mix_send.at[b], mix_recv.at[b], {"tp": peer})
    send_chunks(1)

    hidden = stream_t + mix_s[n_tp - 1].astype(F32)
    for b in range(n_tp - 1):
        arrived(mix_r.at[b], mix_recv.at[b])
        hidden = hidden + mix_r[b].astype(F32)
    hidden_v[...] = hidden
    x_all[sp, tp] = (hidden * norm_gain[...]).astype(BF16)
    own = x_all.at[sp, tp]
    for d in range(1, n_z):
        send(own, own, xs_z.at[d], x_recv.at[sp, tp], {"sp": layers[d] * CORES + core})
    for b, peer in enumerate(peers):
        send(own, own, xs_tp.at[0, b], x_recv.at[sp, tp], {"tp": peer})
    send(own, own, xs_p.at[0, 0], x_recv.at[sp, tp], partner)

    squares = jnp.sum(hidden * hidden, axis=1, keepdims=True)
    row = jnp.broadcast_to(squares, (pos, pos)).T[:SUB]
    ss_s[...] = row
    for b, peer in enumerate(peers):
        send(ss_s, ss_r.at[b], ss_send.at[b], ss_recv.at[b], {"tp": peer})
    send_chunks(2)
    for b in range(n_tp - 1):
        arrived(ss_r.at[b], ss_recv.at[b])
        row = row + ss_r[b]
    scale = lax.rsqrt(row[:1] / width + epsilon)
    meta_r[sp] = jnp.where(at_row == meta_rows - 1, scale, table)
    for d in range(1, n_sp):
        send(meta_r.at[sp], meta_r.at[sp], meta_send.at[d], meta_recv.at[sp],
             {"sp": lax.rem(sp + d, n_sp)})

    def to_partner(slot, b, group):
        block = x_all.at[group, peers[b]]
        arrived(block, x_recv.at[group, peers[b]])
        send(block, block, xs_p.at[slot, b + 1], x_recv.at[group, peers[b]], partner)

    def from_layer(d):
        group = layers[d] * CORES + core
        block = x_all.at[group, tp]
        arrived(block, x_recv.at[group, tp])
        for b, peer in enumerate([] if square and d == 1 else (near if d in along_z else peers)):
            send(block, block, xs_tp.at[d, b], x_recv.at[group, tp], {"tp": peer})
        send(block, block, xs_p.at[d, 0], x_recv.at[group, tp], partner)

    for b in range(n_tp - 1):
        to_partner(0, b, sp)
        if square and b < 2:
            block = x_all.at[sp, peers[b]]
            send(block, block, xs_n.at[b], x_recv.at[sp, peers[b]],
                 {"sp": layers[1] * CORES + core})
    if square:
        block = x_all.at[sp, peers[2]]
        for d in along_z:
            send(block, block, xs_d.at[d], x_recv.at[sp, peers[2]],
                 {"sp": layers[d] * CORES + core})
    from_layer(1)
    send_chunks(3)

    loads[1].wait()
    loads[2].wait()
    scale_own = column_of(scale, pos)[:, :1]
    gate = jnp.zeros((pos, hid), F32)
    upward = jnp.zeros((pos, hid), F32)
    for b in range(n_tp):
        block = x_all[sp, b]
        gate = gate + dot(block, sgate_w[b * feats:(b + 1) * feats, :])
        upward = upward + dot(block, sup_w[b * feats:(b + 1) * feats, :])
    shared_mid = (silu(gate * scale_own) * (upward * scale_own)).astype(BF16)
    loads[3].wait()
    shared_v[...] = dot(shared_mid, sdown_w[...])

    for d in range(2, n_z):
        from_layer(d)
    send_chunks(4)

    loads[4].wait()
    loads[5].wait()
    def widen(d):
        layer = layers[d]
        mine = layer * CORES + core
        other = layer * CORES + 1 - core
        if d > 0:
            for b in range(n_tp - 1):
                to_partner(d, b, mine)
            arrived(meta_r.at[mine], meta_recv.at[mine])
        arrived(meta_r.at[other], meta_recv.at[other])
        for b in range(n_tp):
            arrived(x_all.at[other, b], x_recv.at[other, b])
        gate = jnp.zeros((CORES * pos, hid), F32)
        upward = jnp.zeros((CORES * pos, hid), F32)
        for b in range(n_tp):
            block = x_all[pl.ds(layer * CORES, CORES), b].reshape(CORES * pos, feats)
            gate = gate + dot(block, gate_w[b * feats:(b + 1) * feats, :])
            upward = upward + dot(block, up_w[b * feats:(b + 1) * feats, :])
        scales = jnp.concatenate([
            column_of(meta_r[layer * CORES + i, meta_rows - 1:, :], pos)[:, :1]
            for i in range(CORES)
        ], axis=0)
        mid_v[layer] = (silu(gate * scales) * (upward * scales)).astype(BF16)

    widen(0)
    if n_z > 1:
        widen(1)
    own_down.wait()
    for peer in peers:
        for chunk in range(CHUNKS):
            arrived(down_w.at[peer, pl.ds(chunk * rows, rows), :], wd_recv.at[peer, chunk])

    order = list(range(1, n_z)) + [0]
    half = pos // 2

    def direct(step):
        return square and order[step] == 1

    totals = {}

    def multiply(step):
        layer = layers[order[step]]
        weight = jnp.concatenate([
            column_of(meta_r[layer * CORES + i, pl.ds(sp, 1), :], pos)[:, :1]
            for i in range(CORES)
        ], axis=0)
        middle = mid_v[layer]
        for b in range(n_tp):
            term = dot(middle, down_w[b]) * weight
            lower, upper = term[:pos], term[pos:]
            pr_s[step, b] = jnp.where(core == 0, upper, lower).astype(BF16)
            acc_v[step % 3, b] = jnp.where(core == 0, lower, upper)
        send(pr_s.at[step], pr_r.at[step], pr_send.at[step], pr_recv.at[step], partner)

    def block_of(step, peer):
        term = acc_v[step % 3, peer] + pr_r[step, peer].astype(F32)
        if order[step] == 0:
            cols = pl.ds(pl.multiple_of(peer * feats, feats), feats)
            term = term + shared_v[:, cols]
            if square:
                term = term + rz_r[peer].astype(F32)
        return term

    def cross(step):
        arrived(pr_r.at[step], pr_recv.at[step])
        if direct(step):
            for b in range(n_tp):
                rs_s[step, b] = block_of(step, b).astype(BF16)
            send(rs_s.at[step], rz_r, rz_send, rz_recv, {"sp": layers[1] * CORES + core})
            return
        if square and order[step] == 0:
            arrived(rz_r, rz_recv)
        if square:
            rs_s[step, 2] = block_of(step, peers[2]).astype(BF16)
            for b in range(2):
                part = pl.ds(b * half, half)
                send(rs_s.at[step, 2, part], rd_r.at[step, part], rs_send.at[step, 2 + b],
                     rs_recv.at[step, 2 + b], {"tp": peers[b]})
        rs_s[step, n_tp - 1] = block_of(step, tp).astype(BF16)

    def spread(step):
        if direct(step):
            return
        if square:
            for b in range(2):
                part = pl.ds(b * half, half)
                arrived(rd_r.at[step, part], rs_recv.at[step, 2 + b])
        for b, peer in enumerate(near):
            term = block_of(step, peer)
            if square:
                part = slice((1 - b) * half, (2 - b) * half)
                extra = rd_r[step, part, :].astype(F32)
                fixed = term[b * half:(b + 1) * half]
                joined = [fixed, term[part] + extra]
                term = jnp.concatenate(joined if b == 0 else joined[::-1], axis=0)
            rs_s[step, b] = term.astype(BF16)
            send(rs_s.at[step, b], rs_r.at[step, b], rs_send.at[step, b],
                 rs_recv.at[step, b], {"tp": peer})

    def gathered(step):
        if direct(step):
            return
        total = rs_s[step, n_tp - 1].astype(F32)
        for b in range(len(near)):
            arrived(rs_r.at[step, b], rs_recv.at[step, b])
            total = total + rs_r[step, b].astype(F32)
        d = order[step]
        if d == 0:
            totals[0] = total
        else:
            zr_s[d] = total.astype(BF16)
            send(zr_s.at[d], zr_r.at[d], zr_send.at[d], zr_recv.at[d],
                 {"sp": layers[d] * CORES + core})

    for step in range(n_z + 2):
        if step < n_z:
            multiply(step)
            if step + 2 < n_z:
                widen(step + 2)
        for lag, stage in enumerate((cross, spread, gathered)):
            if 0 <= step - lag < n_z:
                stage(step - lag)

    result = hidden_v[...] + totals[0]
    for d in range(2 if square else 1, n_z):
        arrived(zr_r.at[d], zr_recv.at[d])
        result = result + zr_r[d].astype(F32)
    out[...] = result.T.astype(BF16)
    for copy in pending:
        copy.wait_send()


def local(n_sp, n_tp, *args):
    (stream, values_in, in_gate, out_gate, documents, conv_taps, head_gain, mix_weight,
     norm_gain, routes, route_weight, expert_gate, expert_up, expert_down,
     shared_gate, shared_up, shared_down) = args
    feats, pos = stream.shape
    chans = values_in.shape[0]
    width = feats * n_tp
    hid = expert_gate.shape[2]
    n_z = n_sp // CORES
    meta_rows = -(-(n_sp + 1) // SUB) * SUB
    vmem = pl.BlockSpec(memory_space=pltpu.VMEM)
    anywhere = pl.BlockSpec(memory_space=pl.ANY)
    dma = pltpu.SemaphoreType.DMA
    scratch = [
        pltpu.VMEM((chans, width), BF16),
        pltpu.VMEM((width, hid), BF16),
        pltpu.VMEM((width, hid), BF16),
        pltpu.VMEM((width, hid), BF16),
        pltpu.VMEM((width, hid), BF16),
        pltpu.VMEM((hid, width), BF16),
        pltpu.VMEM((n_tp, hid, feats), BF16),
        pltpu.VMEM((SUB, chans), F32),
        pltpu.VMEM((pos, chans), F32),
        pltpu.VMEM((1, pos), jnp.int32),
        pltpu.VMEM((n_tp, pos, feats), BF16),
        pltpu.VMEM((n_tp, pos, feats), BF16),
        pltpu.VMEM((pos, feats), F32),
        pltpu.VMEM((n_sp, n_tp, pos, feats), BF16),
        pltpu.VMEM((SUB, pos), F32),
        pltpu.VMEM((n_tp, SUB, pos), F32),
        pltpu.VMEM((n_sp, meta_rows, pos), F32),
        pltpu.VMEM((n_z, CORES * pos, hid), BF16),
        pltpu.VMEM((pos, width), F32),
        pltpu.VMEM((3, n_tp, pos, feats), F32),
        pltpu.VMEM((n_z, n_tp, pos, feats), BF16),
        pltpu.VMEM((n_z, n_tp, pos, feats), BF16),
        pltpu.VMEM((n_z, n_tp, pos, feats), BF16),
        pltpu.VMEM((n_z, n_tp, pos, feats), BF16),
        pltpu.VMEM((n_z if n_tp == 4 else 1, pos, feats), BF16),
        pltpu.VMEM((n_tp if n_tp == 4 else 1, pos, feats), BF16),
        pltpu.VMEM((n_z, pos, feats), BF16),
        pltpu.VMEM((n_z, pos, feats), BF16),
        dma((6,)), dma,
        dma((2,)), dma((2,)),
        dma((n_tp,)), dma((n_tp,)),
        dma((n_tp,)), dma((n_tp,)),
        dma((n_sp,)), dma((n_sp,)),
        dma((n_sp, n_tp)),
        dma((n_z, n_tp)), dma((n_z,)), dma((n_z,)), dma((n_tp,)), dma((n_z, n_tp)),
        dma((n_tp, CHUNKS)), dma((n_tp, CHUNKS)),
        dma((n_z,)), dma((n_z,)),
        dma((n_z, n_tp)), dma((n_z, n_tp)),
        dma((n_z,)), dma((n_z,)),
        dma, dma,
    ]
    return pl.pallas_call(
        functools.partial(kernel, n_sp, n_tp),
        out_shape=jax.ShapeDtypeStruct((feats, pos), BF16),
        in_specs=[vmem] * 7 + [anywhere] + [vmem] * 3 + [anywhere] * 6,
        out_specs=vmem,
        scratch_shapes=scratch,
        compiler_params=pltpu.CompilerParams(
            collective_id=0, has_side_effects=True, vmem_limit_bytes=64 * 1024 * 1024 - 65536
        ),
    )(
        stream, values_in, in_gate, out_gate, documents.reshape(1, pos), conv_taps,
        head_gain.reshape(1, chans), mix_weight, norm_gain.reshape(1, feats), routes.T,
        route_weight.T, expert_gate, expert_up, expert_down, shared_gate, shared_up, shared_down,
    )


def solution(mesh):
    in_specs = (
        P("tp", "sp"),
        P("tp", "sp"),
        P("tp", "sp"),
        P("tp", "sp"),
        P("sp"),
        P(None, "tp"),
        P("tp"),
        P("tp", None),
        P("tp"),
        P("sp", None),
        P("sp", None),
        P("sp", None, "tp"),
        P("sp", None, "tp"),
        P("sp", None, "tp"),
        P(None, "tp"),
        P(None, "tp"),
        P("tp", None),
    )
    body = functools.partial(local, mesh.shape["sp"], mesh.shape["tp"])
    return jax.shard_map(
        body, mesh=mesh, in_specs=in_specs, out_specs=P("tp", "sp"), check_vma=False
    )
```

profile of v0, /device:TPU:0, one launch (start us, length us, event | category | flops | bytes accessed | tf_op | source)
XLA Modules:
  0.0 77.6 jit_solution(14276409884369765665)
XLA Ops:
  0.0 76.0 %shard_map.163 = bf16[512,128]{1,0:T(8,128)(2,1)} custom-call(bf16[512,128]{1,0:T(8,128)(2,1)} %stream.1, bf16[256,128]{1,0:T(8,128)(2,1)} %values_in.1, bf16[256,128]{1,0:T(8,128)(2,1)} %in_gate.1, bf16[256,128]{1,0:T(8,128)(2,1)} %out_gate.1, s32[1,128]{1,0:T(1,128)} %bitcast.9, f32[3,256]{1,0:T(4,128)} %conv_taps.1, f32[1,256]{1,0:T(1,128)} %bitcast.8, ...), custom_call_target="tpu_custom_call" | custom-call | tf_op jit(solution)/shard_map/pallas_call | solution.py:434
  76.0 1.6 %copy.19 = bf16[512,128]{1,0:T(8,128)(2,1)} copy(bf16[512,128]{1,0:T(8,128)(2,1)} %shard_map.163) | data formatting | bytes 262144
where the time goes:
time: 78.3 us; the launch traced here: 77.6 us
  Pallas kernels  76 us (97%)
  local copies, waits for them, and re-layouts  1.57 us (2%)
    pallas_call x1, Pallas kernels, local(): pl.pallas_call(functools.partial(kernel, n_sp, n_tp), out_shape=jax.Shape...  76 us
    unnamed x1, local copies, waits for them, and re-layouts  1.57 us

commit v1 on v0

v1 whole, which is shorter than its diff:
```python
import functools

import jax
import jax.numpy as jnp
from jax import lax
from jax.experimental import pallas as pl
from jax.experimental.pallas import tpu as pltpu
from jax.sharding import PartitionSpec as P

HEAD = 64
CORES = 2
SUB = 8
ALONG_Z = (1, 2, 3)
epsilon = 1e-06
MESH = pl.DeviceIdType.MESH
F32 = jnp.float32
BF16 = jnp.bfloat16


def flipped(index, mask):
    bit = 1
    out = index
    while bit <= mask:
        if mask & bit:
            out = out + bit - 2 * bit * lax.rem(lax.div(index, bit), 2)
        bit *= 2
    return out


def dot(left, right):
    return jnp.dot(left, right, preferred_element_type=F32)


def silu(value):
    return value / (1.0 + jnp.exp(-value))


def column_of(row, width):
    return jnp.broadcast_to(row, (width, row.shape[1])).T


def kernel(
    n_sp, n_tp, cap,
    stream, values_in, in_gate, out_gate, documents, conv_taps, head_gain, mix_weight,
    norm_gain, routes, route_weight, expert_gate, expert_up, expert_down,
    shared_gate, shared_up, shared_down,
    out,
    mix_w, gate_w, up_w, sgate_w, sup_w, sdown_w, down_w,
    tail_s, prev_r, prev_docs, mix_s, mix_r, hidden_v, x_all, ss_s, ss_r, meta_r,
    sh_s, sh_r, mid_all, acc_v, pr_s, pr_r, zr_s, zr_r,
    load_sem, halo_send, halo_recv, mix_send, mix_recv, ss_send, ss_recv,
    meta_send, meta_recv, x_recv, xs_tp, xs_z, xs_d, xs_n, xs_p, sh_send, sh_recv,
    mid_send, mid_recv, fwd_send, fwd_recv, pr_send, pr_recv, zr_send, zr_recv,
):
    sp = lax.axis_index("sp")
    tp = lax.axis_index("tp")
    z = lax.div(sp, CORES)
    core = lax.rem(sp, CORES)
    n_z = n_sp // CORES
    feats, pos = stream.shape
    chans = values_in.shape[0]
    width = feats * n_tp
    hid = gate_w.shape[1]
    partner = {"sp": z * CORES + 1 - core}
    peers = [flipped(tp, d) for d in range(1, n_tp)]
    square = n_tp == 4 and n_z > 1
    near = peers[:2] if square else peers
    along_z = [d for d in ALONG_Z if d < n_z] if square else []
    layers = [flipped(z, d) for d in range(n_z)]
    pending = []

    def send(src, dst, ssem, rsem, device):
        copy = pltpu.make_async_remote_copy(
            src_ref=src, dst_ref=dst, send_sem=ssem, recv_sem=rsem,
            device_id=device, device_id_type=MESH,
        )
        copy.start()
        pending.append(copy)

    def arrived(dst, rsem):
        pltpu.make_async_remote_copy(
            src_ref=dst, dst_ref=dst, send_sem=rsem, recv_sem=rsem,
            device_id=partner, device_id_type=MESH,
        ).wait_recv()

    loads = [
        pltpu.make_async_copy(src, dst, load_sem.at[i])
        for i, (src, dst) in enumerate([
            (mix_weight, mix_w), (shared_gate, sgate_w), (shared_up, sup_w),
            (shared_down, sdown_w), (expert_gate.at[0], gate_w), (expert_up.at[0], up_w),
            (expert_down.at[0], down_w),
        ])
    ]
    loads[0].start()

    barrier = pltpu.get_barrier_semaphore()
    for peer in peers:
        pl.semaphore_signal(barrier, inc=1, device_id={"tp": peer}, device_id_type=MESH)
    for d in range(1, n_sp):
        pl.semaphore_signal(
            barrier, inc=1, device_id={"sp": lax.rem(sp + d, n_sp)}, device_id_type=MESH
        )
    with jax.named_scope("barrier"):
        pl.semaphore_wait(barrier, n_tp - 1 + n_sp - 1)

    product = values_in[...].astype(F32) * in_gate[...].astype(F32)
    tail_s[...] = product.T[pos - SUB:, :]
    after = {"sp": lax.rem(sp + 1, n_sp)}
    send(tail_s, prev_r.at[pl.ds(pos - SUB, SUB)], halo_send.at[0], halo_recv.at[0], after)
    send(documents, prev_docs, halo_send.at[1], halo_recv.at[1], after)
    for load in loads[1:]:
        load.start()

    named = routes[...]
    weights = route_weight[...]
    meta_rows = meta_r.shape[1]
    at_row = lax.broadcasted_iota(jnp.int32, (meta_rows, pos), 0)
    table = jnp.zeros((meta_rows, pos), F32)
    for k in range(routes.shape[0]):
        table = table + jnp.where(at_row == named[k:k + 1, :], weights[k:k + 1, :], 0.0)
    taps = [column_of(conv_taps[j:j + 1, :], pos) for j in range(3)]
    stream_t = stream[...].astype(F32).T

    prev_r[: pos - SUB, :] = jnp.zeros((pos - SUB, chans), F32)
    with jax.named_scope("w_halo"):
        arrived(prev_r.at[pl.ds(pos - SUB, SUB)], halo_recv.at[0])
        arrived(prev_docs, halo_recv.at[1])
    before = prev_r[...].T
    docs = documents[...]
    docs_before = jnp.where(sp > 0, prev_docs[...], -1)
    lane_c = lax.broadcasted_iota(jnp.int32, (chans, pos), 1)
    lane_1 = lax.broadcasted_iota(jnp.int32, (1, pos), 1)
    convolved = taps[2] * product
    for shift in (1, 2):
        moved = jnp.where(lane_c < shift, pltpu.roll(before, shift, 1), pltpu.roll(product, shift, 1))
        ids = jnp.where(lane_1 < shift, pltpu.roll(docs_before, shift, 1), pltpu.roll(docs, shift, 1))
        convolved = convolved + jnp.where(ids == docs, taps[2 - shift] * moved, 0.0)
    mixed = out_gate[...].astype(F32) * convolved
    heads = mixed.reshape(chans // HEAD, HEAD, pos)
    heads = heads * lax.rsqrt(jnp.mean(heads * heads, axis=1, keepdims=True) + epsilon)
    heads_t = (heads.reshape(chans, pos).T * head_gain[...]).astype(BF16)

    loads[0].wait()
    for b, peer in enumerate(peers + [tp]):
        cols = pl.ds(pl.multiple_of(peer * feats, feats), feats)
        mix_s[b] = dot(heads_t, mix_w[:, cols]).astype(BF16)
        if b < n_tp - 1:
            send(mix_s.at[b], mix_r.at[b], mix_send.at[b], mix_recv.at[b], {"tp": peer})

    hidden = stream_t + mix_s[n_tp - 1].astype(F32)
    for b in range(n_tp - 1):
        with jax.named_scope(f"w_mix{b}"):
            arrived(mix_r.at[b], mix_recv.at[b])
        hidden = hidden + mix_r[b].astype(F32)
    hidden_v[...] = hidden
    x_all[sp, tp] = (hidden * norm_gain[...]).astype(BF16)
    squares = jnp.sum(hidden * hidden, axis=1, keepdims=True)
    row = jnp.broadcast_to(squares, (pos, pos)).T[:SUB]
    ss_s[...] = row
    for b, peer in enumerate(peers):
        send(ss_s, ss_r.at[b], ss_send.at[b], ss_recv.at[b], {"tp": peer})
    own = x_all.at[sp, tp]
    for b, peer in enumerate(peers):
        send(own, own, xs_tp.at[0, b], x_recv.at[sp, tp], {"tp": peer})
    for d in range(1, n_z):
        send(own, own, xs_z.at[d], x_recv.at[sp, tp], {"sp": layers[d] * CORES + core})
    send(own, own, xs_p.at[0, 0], x_recv.at[sp, tp], partner)

    for b in range(n_tp - 1):
        with jax.named_scope(f"w_ss{b}"):
            arrived(ss_r.at[b], ss_recv.at[b])
        row = row + ss_r[b]
    scale = lax.rsqrt(row[:1] / width + epsilon)
    meta_r[sp] = jnp.where(at_row == meta_rows - 1, scale, table)
    for d in range(1, n_sp):
        send(meta_r.at[sp], meta_r.at[sp], meta_send.at[d], meta_recv.at[sp],
             {"sp": lax.rem(sp + d, n_sp)})

    def to_partner(slot, b, group):
        block = x_all.at[group, peers[b]]
        with jax.named_scope(f"w_x{slot}_{b}"):
            arrived(block, x_recv.at[group, peers[b]])
        send(block, block, xs_p.at[slot, b + 1], x_recv.at[group, peers[b]], partner)

    def from_layer(d):
        group = layers[d] * CORES + core
        block = x_all.at[group, tp]
        with jax.named_scope(f"w_layer{d}"):
            arrived(block, x_recv.at[group, tp])
        for b, peer in enumerate([] if square and d == 1 else (near if d in along_z else peers)):
            send(block, block, xs_tp.at[d, b], x_recv.at[group, tp], {"tp": peer})
        send(block, block, xs_p.at[d, 0], x_recv.at[group, tp], partner)

    for b in range(n_tp - 1):
        to_partner(0, b, sp)
        if square and b < 2:
            block = x_all.at[sp, peers[b]]
            send(block, block, xs_n.at[b], x_recv.at[sp, peers[b]],
                 {"sp": layers[1] * CORES + core})
    if square:
        block = x_all.at[sp, peers[2]]
        for d in along_z:
            send(block, block, xs_d.at[d], x_recv.at[sp, peers[2]],
                 {"sp": layers[d] * CORES + core})
    if n_z > 1:
        from_layer(1)

    with jax.named_scope("w_load"):
        for i in (1, 2, 3):
            loads[i].wait()
    scale_own = column_of(scale, pos)[:, :1]
    gate = jnp.zeros((pos, hid), F32)
    upward = jnp.zeros((pos, hid), F32)
    for b in range(n_tp):
        block = x_all[sp, b]
        gate = gate + dot(block, sgate_w[b * feats:(b + 1) * feats, :])
        upward = upward + dot(block, sup_w[b * feats:(b + 1) * feats, :])
    shared_mid = (silu(gate * scale_own) * (upward * scale_own)).astype(BF16)
    for b, peer in enumerate(peers + [tp]):
        cols = pl.ds(pl.multiple_of(peer * feats, feats), feats)
        sh_s[b] = dot(shared_mid, sdown_w[:, cols]).astype(BF16)
        if b < n_tp - 1:
            send(sh_s.at[b], sh_r.at[b], sh_send.at[b], sh_recv.at[b], {"tp": peer})

    for d in range(2, n_z):
        from_layer(d)

    with jax.named_scope("w_load2"):
        for i in (4, 5, 6):
            loads[i].wait()

    at_a = lax.broadcasted_iota(jnp.int32, (pos, pos), 0)
    at_b = lax.broadcasted_iota(jnp.int32, (pos, pos), 1)
    earlier = jnp.where(at_a < at_b, 1.0, 0.0).astype(BF16)
    rank_row = lax.broadcasted_iota(jnp.int32, (cap, pos), 0).astype(F32)
    rank_lane = lax.broadcasted_iota(jnp.int32, (pos, cap), 1).astype(F32)

    def groups_of(d):
        return layers[d] * CORES + core, layers[d] * CORES + 1 - core

    def slots_of(group):
        weight = meta_r[group, pl.ds(sp, 1), :]
        mask = jnp.where(weight > 0.0, 1.0, 0.0)
        count = dot(jnp.broadcast_to(mask, (2 * SUB, pos)).astype(BF16), earlier)[:1]
        return weight, jnp.where(weight > 0.0, count, -1.0)

    def widen(d):
        mine, other = groups_of(d)
        if d > 0:
            for b in range(n_tp - 1):
                to_partner(d, b, mine)
            with jax.named_scope(f"w_meta{d}"):
                arrived(meta_r.at[mine], meta_recv.at[mine])
        with jax.named_scope(f"w_other{d}"):
            arrived(meta_r.at[other], meta_recv.at[other])
            for b in range(n_tp):
                arrived(x_all.at[other, b], x_recv.at[other, b])
        gate = jnp.zeros((CORES * pos, hid), F32)
        upward = jnp.zeros((CORES * pos, hid), F32)
        for b in range(n_tp):
            block = jnp.concatenate([x_all[mine, b], x_all[other, b]], axis=0)
            gate = gate + dot(block, gate_w[b * feats:(b + 1) * feats, :])
            upward = upward + dot(block, up_w[b * feats:(b + 1) * feats, :])
        scales = jnp.concatenate([
            column_of(meta_r[group, meta_rows - 1:, :], pos)[:, :1] for group in (mine, other)
        ], axis=0)
        middle = (silu(gate * scales) * (upward * scales)).astype(BF16)
        for i, group in enumerate((mine, other)):
            slot = slots_of(group)[1]
            pick = jnp.where(rank_row == slot, 1.0, 0.0).astype(BF16)
            mid_all[d, tp, i * cap:(i + 1) * cap, :] = dot(
                pick, middle[i * pos:(i + 1) * pos]
            ).astype(BF16)
        block = mid_all.at[d, tp]
        for b, peer in enumerate(near):
            send(block, block, mid_send.at[d, b], mid_recv.at[d, tp], {"tp": peer})

    def relay(d):
        for b, peer in enumerate(near):
            with jax.named_scope(f"w_mid{d}_{b}"):
                arrived(mid_all.at[d, peer], mid_recv.at[d, peer])
            if square:
                part = mid_all.at[d, peer, pl.ds(b * cap, cap)]
                send(part, part, fwd_send.at[d, b], fwd_recv.at[d, b], {"tp": near[1 - b]})

    def narrow(d):
        if square:
            for b in range(2):
                with jax.named_scope(f"w_fwd{d}_{b}"):
                    arrived(mid_all.at[d, peers[2], pl.ds(b * cap, cap)], fwd_recv.at[d, b])
        total = jnp.zeros((CORES * cap, feats), F32)
        for b in range(n_tp):
            total = total + dot(mid_all[d, b], down_w[b * hid:(b + 1) * hid, :])
        total = total.astype(BF16)
        terms = []
        for i, group in enumerate(groups_of(d)):
            weight, slot = slots_of(group)
            place = jnp.where(rank_lane == column_of(slot, cap), 1.0, 0.0).astype(BF16)
            term = dot(place, total[i * cap:(i + 1) * cap])
            terms.append(term * column_of(weight, pos)[:, :1])
        acc_v[d] = terms[0]
        pr_s[d] = terms[1].astype(BF16)
        send(pr_s.at[d], pr_r.at[d], pr_send.at[d], pr_recv.at[d], partner)

    def join(d):
        with jax.named_scope(f"w_pr{d}"):
            arrived(pr_r.at[d], pr_recv.at[d])
        if d > 0:
            zr_s[d] = (acc_v[d] + pr_r[d].astype(F32)).astype(BF16)
            send(zr_s.at[d], zr_r.at[d], zr_send.at[d], zr_recv.at[d],
                 {"sp": layers[d] * CORES + core})

    order = list(range(1, n_z)) + [0]
    for step in range(n_z + 3):
        for lag, stage in enumerate((widen, relay, narrow, join)):
            if 0 <= step - lag < n_z:
                stage(order[step - lag])

    result = hidden_v[...] + sh_s[n_tp - 1].astype(F32)
    for b in range(n_tp - 1):
        with jax.named_scope(f"w_sh{b}"):
            arrived(sh_r.at[b], sh_recv.at[b])
        result = result + sh_r[b].astype(F32)
    result = result + acc_v[0] + pr_r[0].astype(F32)
    for d in range(1, n_z):
        with jax.named_scope(f"w_zr{d}"):
            arrived(zr_r.at[d], zr_recv.at[d])
        result = result + zr_r[d].astype(F32)
    out[...] = result.T.astype(BF16)
    with jax.named_scope("w_send"):
        for copy in pending:
            copy.wait_send()


def local(n_sp, n_tp, *args):
    (stream, values_in, in_gate, out_gate, documents, conv_taps, head_gain, mix_weight,
     norm_gain, routes, route_weight, expert_gate, expert_up, expert_down,
     shared_gate, shared_up, shared_down) = args
    feats, pos = stream.shape
    chans = values_in.shape[0]
    width = feats * n_tp
    hid = expert_gate.shape[2]
    n_z = n_sp // CORES
    meta_rows = -(-(n_sp + 1) // SUB) * SUB
    experts = n_sp * expert_gate.shape[0]
    bound = 3 * pos * routes.shape[1] // (2 * experts)
    cap = -(-bound // (2 * SUB)) * 2 * SUB
    vmem = pl.BlockSpec(memory_space=pltpu.VMEM)
    anywhere = pl.BlockSpec(memory_space=pl.ANY)
    dma = pltpu.SemaphoreType.DMA
    scratch = [
        pltpu.VMEM((chans, width), BF16),
        pltpu.VMEM((width, hid), BF16),
        pltpu.VMEM((width, hid), BF16),
        pltpu.VMEM((width, hid), BF16),
        pltpu.VMEM((width, hid), BF16),
        pltpu.VMEM((hid, width), BF16),
        pltpu.VMEM((n_tp * hid, feats), BF16),
        pltpu.VMEM((SUB, chans), F32),
        pltpu.VMEM((pos, chans), F32),
        pltpu.VMEM((1, pos), jnp.int32),
        pltpu.VMEM((n_tp, pos, feats), BF16),
        pltpu.VMEM((n_tp, pos, feats), BF16),
        pltpu.VMEM((pos, feats), F32),
        pltpu.VMEM((n_sp, n_tp, pos, feats), BF16),
        pltpu.VMEM((SUB, pos), F32),
        pltpu.VMEM((n_tp, SUB, pos), F32),
        pltpu.VMEM((n_sp, meta_rows, pos), F32),
        pltpu.VMEM((n_tp, pos, feats), BF16),
        pltpu.VMEM((n_tp, pos, feats), BF16),
        pltpu.VMEM((n_z, n_tp, CORES * cap, hid), BF16),
        pltpu.VMEM((n_z, pos, feats), F32),
        pltpu.VMEM((n_z, pos, feats), BF16),
        pltpu.VMEM((n_z, pos, feats), BF16),
        pltpu.VMEM((n_z, pos, feats), BF16),
        pltpu.VMEM((n_z, pos, feats), BF16),
        dma((7,)),
        dma((2,)), dma((2,)),
        dma((n_tp,)), dma((n_tp,)),
        dma((n_tp,)), dma((n_tp,)),
        dma((n_sp,)), dma((n_sp,)),
        dma((n_sp, n_tp)),
        dma((n_z, n_tp)), dma((n_z,)), dma((n_z,)), dma((n_tp,)), dma((n_z, n_tp)),
        dma((n_tp,)), dma((n_tp,)),
        dma((n_z, n_tp)), dma((n_z, n_tp)),
        dma((n_z, 2)), dma((n_z, 2)),
        dma((n_z,)), dma((n_z,)),
        dma((n_z,)), dma((n_z,)),
    ]
    return pl.pallas_call(
        functools.partial(kernel, n_sp, n_tp, cap),
        out_shape=jax.ShapeDtypeStruct((feats, pos), BF16),
        in_specs=[vmem] * 7 + [anywhere] + [vmem] * 3 + [anywhere] * 6,
        out_specs=vmem,
        scratch_shapes=scratch,
        compiler_params=pltpu.CompilerParams(
            collective_id=0, has_side_effects=True, vmem_limit_bytes=64 * 1024 * 1024 - 65536
        ),
    )(
        stream, values_in, in_gate, out_gate, documents.reshape(1, pos), conv_taps,
        head_gain.reshape(1, chans), mix_weight, norm_gain.reshape(1, feats), routes.T,
        route_weight.T, expert_gate, expert_up, expert_down, shared_gate, shared_up, shared_down,
    )


def solution(mesh):
    in_specs = (
        P("tp", "sp"),
        P("tp", "sp"),
        P("tp", "sp"),
        P("tp", "sp"),
        P("sp"),
        P(None, "tp"),
        P("tp"),
        P("tp", None),
        P("tp"),
        P("sp", None),
        P("sp", None),
        P("sp", None, "tp"),
        P("sp", None, "tp"),
        P("sp", None, "tp"),
        P(None, "tp"),
        P(None, "tp"),
        P("tp", None),
    )
    body = functools.partial(local, mesh.shape["sp"], mesh.shape["tp"])
    return jax.shard_map(
        body, mesh=mesh, in_specs=in_specs, out_specs=P("tp", "sp"), check_vma=False
    )
```

time: 78.3 us -> 81.3 us (1.038)
  Pallas kernels: 76 us -> 79.2 us
    pallas_call x1, Pallas kernels: 76 us -> 79.2 us  [local(): pl.pallas_call(functools.partial(kernel, n_sp, n_tp, cap), out_shape=jax....]
where the time goes in v1:
time: 81.3 us; the launch traced here: 80.8 us
  Pallas kernels  79.2 us (97%)
  local copies, waits for them, and re-layouts  1.57 us (2%)
    pallas_call x1, Pallas kernels, local(): pl.pallas_call(functools.partial(kernel, n_sp, n_tp, cap), out_shape=jax....  79.2 us

profile of v1, /device:TPU:0, one launch (start us, length us, event | category | flops | bytes accessed | tf_op | source)
XLA Modules:
  0.0 80.8 jit_solution(9366884367931525461)
XLA Ops:
  0.0 79.2 %shard_map.163 = bf16[512,128]{1,0:T(8,128)(2,1)} custom-call(bf16[512,128]{1,0:T(8,128)(2,1)} %stream.1, bf16[256,128]{1,0:T(8,128)(2,1)} %values_in.1, bf16[256,128]{1,0:T(8,128)(2,1)} %in_gate.1, bf16[256,128]{1,0:T(8,128)(2,1)} %out_gate.1, s32[1,128]{1,0:T(1,128)} %bitcast.9, f32[3,256]{1,0:T(4,128)} %conv_taps.1, f32[1,256]{1,0:T(1,128)} %bitcast.8, ...), custom_call_target="tpu_custom_call" | custom-call | tf_op jit(solution)/shard_map/pallas_call | solution.py:390
  79.3 1.6 %copy.19 = bf16[512,128]{1,0:T(8,128)(2,1)} copy(bf16[512,128]{1,0:T(8,128)(2,1)} %shard_map.163) | data formatting | bytes 262144

commit v2 on v1

--- a/solution.py
+++ b/solution.py
@@ -10,7 +10,7 @@
 HEAD = 64
 CORES = 2
 SUB = 8
-ALONG_Z = (1, 2, 3)
+EDGE = 16
 epsilon = 1e-06
 MESH = pl.DeviceIdType.MESH
 F32 = jnp.float32
@@ -41,15 +41,16 @@
 
 def kernel(
     n_sp, n_tp, cap,
-    stream, values_in, in_gate, out_gate, documents, conv_taps, head_gain, mix_weight,
-    norm_gain, routes, route_weight, expert_gate, expert_up, expert_down,
+    stream_h, values_h, in_h, out_h, documents_h, taps_h, head_h, mix_weight,
+    norm_h, routes_h, route_weight_h, expert_gate, expert_up, expert_down,
     shared_gate, shared_up, shared_down,
     out,
-    mix_w, gate_w, up_w, sgate_w, sup_w, sdown_w, down_w,
+    stream, values_in, in_gate, out_gate, documents, conv_taps, head_gain,
+    norm_gain, routes, route_weight, mix_w, gate_w, up_w, sgate_w, sup_w, sdown_w, down_w,
     tail_s, prev_r, prev_docs, mix_s, mix_r, hidden_v, x_all, ss_s, ss_r, meta_r,
     sh_s, sh_r, mid_all, acc_v, pr_s, pr_r, zr_s, zr_r,
-    load_sem, halo_send, halo_recv, mix_send, mix_recv, ss_send, ss_recv,
-    meta_send, meta_recv, x_recv, xs_tp, xs_z, xs_d, xs_n, xs_p, sh_send, sh_recv,
+    small_sem, load_sem, halo_send, halo_recv, mix_send, mix_recv, ss_send, ss_recv,
+    meta_send, meta_recv, x_recv, xs_tp, xs_z, xs_r, xs_n, xs_p, sh_send, sh_recv,
     mid_send, mid_recv, fwd_send, fwd_recv, pr_send, pr_recv, zr_send, zr_recv,
 ):
     sp = lax.axis_index("sp")
@@ -63,19 +64,36 @@
     hid = gate_w.shape[1]
     partner = {"sp": z * CORES + 1 - core}
     peers = [flipped(tp, d) for d in range(1, n_tp)]
-    square = n_tp == 4 and n_z > 1
+    square = n_tp == 4 and n_z == 4
     near = peers[:2] if square else peers
-    along_z = [d for d in ALONG_Z if d < n_z] if square else []
     layers = [flipped(z, d) for d in range(n_z)]
     pending = []
+    inner = lax.div(z + 1, 2) == 1
+    if square:
+        layers[2:] = [jnp.where(inner, layers[3], layers[2]), jnp.where(inner, layers[2], layers[3])]
+    turns = {"inner": [], "end": []}
+
+    def only(where, stage, *args):
+        @pl.when(inner if where == "inner" else jnp.logical_not(inner))
+        def _():
+            kept = len(pending)
+            stage(*args)
+            turns[where].extend((sem, size) for _, sem, size in pending[kept:])
+            del pending[kept:]
+
+    def onward(block, rsem, slot, d):
+        def relay_on():
+            send(block, block, (xs_r, slot, d), rsem, {"sp": layers[2 if d < 2 else 1] * CORES + core})
+        return relay_on
 
     def send(src, dst, ssem, rsem, device):
+        sem = ssem[0].at[ssem[1:]] if isinstance(ssem, tuple) else ssem
         copy = pltpu.make_async_remote_copy(
-            src_ref=src, dst_ref=dst, send_sem=ssem, recv_sem=rsem,
+            src_ref=src, dst_ref=dst, send_sem=sem, recv_sem=rsem,
             device_id=device, device_id_type=MESH,
         )
         copy.start()
-        pending.append(copy)
+        pending.append((copy, ssem, src.shape))
 
     def arrived(dst, rsem):
         pltpu.make_async_remote_copy(
@@ -91,7 +109,14 @@
             (expert_down.at[0], down_w),
         ])
     ]
-    loads[0].start()
+    smalls = [
+        pltpu.make_async_copy(src, dst, small_sem.at[i])
+        for i, (src, dst) in enumerate([
+            (values_h, values_in), (in_h, in_gate), (documents_h, documents), (out_h, out_gate),
+            (taps_h, conv_taps), (head_h, head_gain), (routes_h, routes),
+            (route_weight_h, route_weight), (stream_h, stream), (norm_h, norm_gain),
+        ])
+    ]
 
     barrier = pltpu.get_barrier_semaphore()
     for peer in peers:
@@ -100,16 +125,86 @@
         pl.semaphore_signal(
             barrier, inc=1, device_id={"sp": lax.rem(sp + d, n_sp)}, device_id_type=MESH
         )
+    for copy in smalls:
+        copy.start()
+    loads[0].start()
+    for copy in smalls[:3]:
+        copy.wait()
+    product = values_in[...].astype(F32) * in_gate[...].astype(F32)
+    tail_s[...] = product.T[pos - SUB:, :]
+    for copy in smalls[3:]:
+        copy.wait()
+
+    tap_rows = jnp.concatenate([conv_taps[...], jnp.zeros((SUB - 3, chans), F32)], axis=0).T
+    taps = [jnp.broadcast_to(tap_rows[:, j:j + 1], (chans, pos)) for j in range(3)]
+    docs = documents[...]
+    lane_c = lax.broadcasted_iota(jnp.int32, (chans, pos), 1)
+    lane_1 = lax.broadcasted_iota(jnp.int32, (1, pos), 1)
+
+    def heads_of(before, docs_before):
+        convolved = taps[2] * product
+        for shift in (1, 2):
+            moved = pltpu.roll(product, shift, 1)
+            if before is not None:
+                moved = jnp.where(lane_c < shift, pltpu.roll(before, shift, 1), moved)
+            ids = jnp.where(lane_1 < shift, pltpu.roll(docs_before, shift, 1), pltpu.roll(docs, shift, 1))
+            convolved = convolved + jnp.where(ids == docs, taps[2 - shift] * moved, 0.0)
+        mixed = out_gate[...].astype(F32) * convolved
+        heads = mixed.reshape(chans // HEAD, HEAD, pos)
+        heads = heads * lax.rsqrt(jnp.mean(heads * heads, axis=1, keepdims=True) + epsilon)
+        return (heads.reshape(chans, pos).T * head_gain[...]).astype(BF16)
+
+    def mix(rows, heads_t):
+        for b, peer in enumerate(peers + [tp]):
+            cols = pl.ds(pl.multiple_of(peer * feats, feats), feats)
+            mix_s[b, rows[0]:rows[1]] = dot(heads_t[rows[0]:rows[1]], mix_w[:, cols]).astype(BF16)
+
+    def send_mix(rows, stage):
+        part = pl.ds(rows[0], rows[1] - rows[0])
+        for b, peer in enumerate(peers):
+            send(mix_s.at[b, part], mix_r.at[b, part], mix_send.at[stage, b],
+                 mix_recv.at[stage, b], {"tp": peer})
+
+    heads_t = heads_of(None, jnp.full((1, pos), -1, jnp.int32))
+    loads[0].wait()
+    for load in loads[1:]:
+        load.start()
+    mix((EDGE, pos), heads_t)
     with jax.named_scope("barrier"):
         pl.semaphore_wait(barrier, n_tp - 1 + n_sp - 1)
-
-    product = values_in[...].astype(F32) * in_gate[...].astype(F32)
-    tail_s[...] = product.T[pos - SUB:, :]
     after = {"sp": lax.rem(sp + 1, n_sp)}
-    send(tail_s, prev_r.at[pl.ds(pos - SUB, SUB)], halo_send.at[0], halo_recv.at[0], after)
-    send(documents, prev_docs, halo_send.at[1], halo_recv.at[1], after)
-    for load in loads[1:]:
-        load.start()
+    halo = [
+        pltpu.make_async_remote_copy(
+            src_ref=src, dst_ref=dst, send_sem=halo_send.at[i], recv_sem=halo_recv.at[i],
+            device_id=after, device_id_type=MESH,
+        )
+        for i, (src, dst) in enumerate([
+            (tail_s, prev_r.at[pl.ds(pos - SUB, SUB)]), (documents, prev_docs),
+        ])
+    ]
+
+    @pl.when(sp < n_sp - 1)
+    def _():
+        for copy in halo:
+            copy.start()
+
+    send_mix((EDGE, pos), 0)
+
+    @pl.when(sp == 0)
+    def _():
+        prev_r[...] = jnp.zeros((pos, chans), F32)
+        prev_docs[...] = jnp.full((1, pos), -1, jnp.int32)
+
+    @pl.when(sp > 0)
+    def _():
+        prev_r[: pos - SUB, :] = jnp.zeros((pos - SUB, chans), F32)
+        with jax.named_scope("w_halo"):
+            for copy in halo:
+                copy.wait_recv()
+
+    heads_t = heads_of(prev_r[...].T, prev_docs[...])
+    mix((0, EDGE), heads_t)
+    send_mix((0, EDGE), 1)
 
     named = routes[...]
     weights = route_weight[...]
@@ -118,39 +213,13 @@
     table = jnp.zeros((meta_rows, pos), F32)
     for k in range(routes.shape[0]):
         table = table + jnp.where(at_row == named[k:k + 1, :], weights[k:k + 1, :], 0.0)
-    taps = [column_of(conv_taps[j:j + 1, :], pos) for j in range(3)]
     stream_t = stream[...].astype(F32).T
-
-    prev_r[: pos - SUB, :] = jnp.zeros((pos - SUB, chans), F32)
-    with jax.named_scope("w_halo"):
-        arrived(prev_r.at[pl.ds(pos - SUB, SUB)], halo_recv.at[0])
-        arrived(prev_docs, halo_recv.at[1])
-    before = prev_r[...].T
-    docs = documents[...]
-    docs_before = jnp.where(sp > 0, prev_docs[...], -1)
-    lane_c = lax.broadcasted_iota(jnp.int32, (chans, pos), 1)
-    lane_1 = lax.broadcasted_iota(jnp.int32, (1, pos), 1)
-    convolved = taps[2] * product
-    for shift in (1, 2):
-        moved = jnp.where(lane_c < shift, pltpu.roll(before, shift, 1), pltpu.roll(product, shift, 1))
-        ids = jnp.where(lane_1 < shift, pltpu.roll(docs_before, shift, 1), pltpu.roll(docs, shift, 1))
-        convolved = convolved + jnp.where(ids == docs, taps[2 - shift] * moved, 0.0)
-    mixed = out_gate[...].astype(F32) * convolved
-    heads = mixed.reshape(chans // HEAD, HEAD, pos)
-    heads = heads * lax.rsqrt(jnp.mean(heads * heads, axis=1, keepdims=True) + epsilon)
-    heads_t = (heads.reshape(chans, pos).T * head_gain[...]).astype(BF16)
-
-    loads[0].wait()
-    for b, peer in enumerate(peers + [tp]):
-        cols = pl.ds(pl.multiple_of(peer * feats, feats), feats)
-        mix_s[b] = dot(heads_t, mix_w[:, cols]).astype(BF16)
-        if b < n_tp - 1:
-            send(mix_s.at[b], mix_r.at[b], mix_send.at[b], mix_recv.at[b], {"tp": peer})
 
     hidden = stream_t + mix_s[n_tp - 1].astype(F32)
     for b in range(n_tp - 1):
         with jax.named_scope(f"w_mix{b}"):
-            arrived(mix_r.at[b], mix_recv.at[b])
+            arrived(mix_r.at[b, pl.ds(EDGE, pos - EDGE)], mix_recv.at[0, b])
+            arrived(mix_r.at[b, pl.ds(0, EDGE)], mix_recv.at[1, b])
         hidden = hidden + mix_r[b].astype(F32)
     hidden_v[...] = hidden
     x_all[sp, tp] = (hidden * norm_gain[...]).astype(BF16)
@@ -161,10 +230,12 @@
         send(ss_s, ss_r.at[b], ss_send.at[b], ss_recv.at[b], {"tp": peer})
     own = x_all.at[sp, tp]
     for b, peer in enumerate(peers):
-        send(own, own, xs_tp.at[0, b], x_recv.at[sp, tp], {"tp": peer})
-    for d in range(1, n_z):
-        send(own, own, xs_z.at[d], x_recv.at[sp, tp], {"sp": layers[d] * CORES + core})
-    send(own, own, xs_p.at[0, 0], x_recv.at[sp, tp], partner)
+        send(own, own, (xs_tp, 0, b), x_recv.at[sp, tp], {"tp": peer})
+    for d in ([1] if square else range(1, n_z)):
+        send(own, own, (xs_z, d), x_recv.at[sp, tp], {"sp": layers[d] * CORES + core})
+    if square:
+        only("inner", onward(own, x_recv.at[sp, tp], 0, 0))
+    send(own, own, (xs_p, 0, 0), x_recv.at[sp, tp], partner)
 
     for b in range(n_tp - 1):
         with jax.named_scope(f"w_ss{b}"):
@@ -180,41 +251,50 @@
         block = x_all.at[group, peers[b]]
         with jax.named_scope(f"w_x{slot}_{b}"):
             arrived(block, x_recv.at[group, peers[b]])
-        send(block, block, xs_p.at[slot, b + 1], x_recv.at[group, peers[b]], partner)
+        send(block, block, (xs_p, slot, b + 1), x_recv.at[group, peers[b]], partner)
 
     def from_layer(d):
         group = layers[d] * CORES + core
         block = x_all.at[group, tp]
         with jax.named_scope(f"w_layer{d}"):
             arrived(block, x_recv.at[group, tp])
-        for b, peer in enumerate([] if square and d == 1 else (near if d in along_z else peers)):
-            send(block, block, xs_tp.at[d, b], x_recv.at[group, tp], {"tp": peer})
-        send(block, block, xs_p.at[d, 0], x_recv.at[group, tp], partner)
-
-    for b in range(n_tp - 1):
-        to_partner(0, b, sp)
-        if square and b < 2:
-            block = x_all.at[sp, peers[b]]
-            send(block, block, xs_n.at[b], x_recv.at[sp, peers[b]],
-                 {"sp": layers[1] * CORES + core})
+        for b, peer in enumerate([] if square and d != 2 else near):
+            send(block, block, (xs_tp, d, b), x_recv.at[group, tp], {"tp": peer})
+        send(block, block, (xs_p, d, 0), x_recv.at[group, tp], partner)
+
+    def closer(b):
+        block = x_all.at[sp, peers[b]]
+        send(block, block, (xs_n, b), x_recv.at[sp, peers[b]], {"sp": layers[1] * CORES + core})
+
+    def from_layer_inner(d):
+        group = layers[d] * CORES + core
+        from_layer(d)
+        onward(x_all.at[group, tp], x_recv.at[group, tp], 0, d)()
+
     if square:
-        block = x_all.at[sp, peers[2]]
-        for d in along_z:
-            send(block, block, xs_d.at[d], x_recv.at[sp, peers[2]],
-                 {"sp": layers[d] * CORES + core})
-    if n_z > 1:
-        from_layer(1)
+        only("inner", from_layer_inner, 1)
+        only("inner", from_layer_inner, 2)
 
     with jax.named_scope("w_load"):
         for i in (1, 2, 3):
             loads[i].wait()
     scale_own = column_of(scale, pos)[:, :1]
-    gate = jnp.zeros((pos, hid), F32)
-    upward = jnp.zeros((pos, hid), F32)
-    for b in range(n_tp):
-        block = x_all[sp, b]
-        gate = gate + dot(block, sgate_w[b * feats:(b + 1) * feats, :])
-        upward = upward + dot(block, sup_w[b * feats:(b + 1) * feats, :])
+
+    def shared_part(peer):
+        rows = pl.ds(pl.multiple_of(peer * feats, feats), feats)
+        block = x_all[sp, peer]
+        return dot(block, sgate_w[rows, :]), dot(block, sup_w[rows, :])
+
+    gate, upward = shared_part(tp)
+    for b in range(n_tp - 1):
+        to_partner(0, b, sp)
+        block = x_all.at[sp, peers[b]]
+        if square:
+            closer(b)
+        if square and b == 2:
+            only("inner", onward(block, x_recv.at[sp, peers[2]], 3, 0))
+        more = shared_part(peers[b])
+        gate, upward = gate + more[0], upward + more[1]
     shared_mid = (silu(gate * scale_own) * (upward * scale_own)).astype(BF16)
     for b, peer in enumerate(peers + [tp]):
         cols = pl.ds(pl.multiple_of(peer * feats, feats), feats)
@@ -222,9 +302,6 @@
         if b < n_tp - 1:
             send(sh_s.at[b], sh_r.at[b], sh_send.at[b], sh_recv.at[b], {"tp": peer})
 
-    for d in range(2, n_z):
-        from_layer(d)
-
     with jax.named_scope("w_load2"):
         for i in (4, 5, 6):
             loads[i].wait()
@@ -244,14 +321,20 @@
         count = dot(jnp.broadcast_to(mask, (2 * SUB, pos)).astype(BF16), earlier)[:1]
         return weight, jnp.where(weight > 0.0, count, -1.0)
 
+    def fetch(d, b):
+        to_partner(d, b, groups_of(d)[0])
+
+    def fetch_inner(d, b):
+        group = groups_of(d)[0]
+        to_partner(d, b, group)
+        block = x_all.at[group, peers[b]]
+        onward(block, x_recv.at[group, peers[b]], b + 1, d)()
+
     def widen(d):
         mine, other = groups_of(d)
-        if d > 0:
-            for b in range(n_tp - 1):
-                to_partner(d, b, mine)
-            with jax.named_scope(f"w_meta{d}"):
+        with jax.named_scope(f"w_other{d}"):
+            if d > 0:
                 arrived(meta_r.at[mine], meta_recv.at[mine])
-        with jax.named_scope(f"w_other{d}"):
             arrived(meta_r.at[other], meta_recv.at[other])
             for b in range(n_tp):
                 arrived(x_all.at[other, b], x_recv.at[other, b])
@@ -271,17 +354,19 @@
             mid_all[d, tp, i * cap:(i + 1) * cap, :] = dot(
                 pick, middle[i * pos:(i + 1) * pos]
             ).astype(BF16)
-        block = mid_all.at[d, tp]
+
+    def mids(d, i):
+        block = mid_all.at[d, tp, pl.ds(i * cap, cap)]
         for b, peer in enumerate(near):
-            send(block, block, mid_send.at[d, b], mid_recv.at[d, tp], {"tp": peer})
-
-    def relay(d):
+            send(block, block, (mid_send, d, i, b), mid_recv.at[d, i, tp], {"tp": peer})
+
+    def relay(d, i):
         for b, peer in enumerate(near):
-            with jax.named_scope(f"w_mid{d}_{b}"):
-                arrived(mid_all.at[d, peer], mid_recv.at[d, peer])
-            if square:
-                part = mid_all.at[d, peer, pl.ds(b * cap, cap)]
-                send(part, part, fwd_send.at[d, b], fwd_recv.at[d, b], {"tp": near[1 - b]})
+            part = mid_all.at[d, peer, pl.ds(i * cap, cap)]
+            with jax.named_scope(f"w_mid{d}_{i}_{b}"):
+                arrived(part, mid_recv.at[d, i, peer])
+            if square and b == i:
+                send(part, part, (fwd_send, d, i), fwd_recv.at[d, i], {"tp": near[1 - b]})
 
     def narrow(d):
         if square:
@@ -300,21 +385,46 @@
             terms.append(term * column_of(weight, pos)[:, :1])
         acc_v[d] = terms[0]
         pr_s[d] = terms[1].astype(BF16)
-        send(pr_s.at[d], pr_r.at[d], pr_send.at[d], pr_recv.at[d], partner)
+        send(pr_s.at[d], pr_r.at[d], (pr_send, d), pr_recv.at[d], partner)
 
     def join(d):
         with jax.named_scope(f"w_pr{d}"):
             arrived(pr_r.at[d], pr_recv.at[d])
         if d > 0:
             zr_s[d] = (acc_v[d] + pr_r[d].astype(F32)).astype(BF16)
-            send(zr_s.at[d], zr_r.at[d], zr_send.at[d], zr_recv.at[d],
+            send(zr_s.at[d], zr_r.at[z], (zr_send, d), zr_recv.at[z],
                  {"sp": layers[d] * CORES + core})
 
-    order = list(range(1, n_z)) + [0]
-    for step in range(n_z + 3):
-        for lag, stage in enumerate((widen, relay, narrow, join)):
-            if 0 <= step - lag < n_z:
-                stage(order[step - lag])
+    def run(plan):
+        for stage, *where in plan:
+            stage(*where)
+
+    if square:
+        plan = [(from_layer, 1), (widen, 0), (mids, 0, 0), (from_layer, 2), (mids, 0, 1)]
+        plan += [(fetch, 1, b) for b in range(3)] + [(widen, 1), (mids, 1, 0), (mids, 1, 1)]
+        plan += [(relay, 0, 0), (relay, 0, 1), (from_layer, 3)]
+        plan += [(fetch, 2, b) for b in range(3)] + [(widen, 2), (mids, 2, 0), (mids, 2, 1)]
+        plan += [(relay, 1, 0), (relay, 1, 1), (relay, 2, 0)]
+        plan += [(fetch, 3, b) for b in range(3)] + [(widen, 3), (mids, 3, 0), (mids, 3, 1)]
+        plan += [(relay, 2, 1), (narrow, 1), (relay, 3, 0), (join, 1), (relay, 3, 1)]
+        plan += [(narrow, 2), (join, 2), (narrow, 0), (narrow, 3), (join, 3), (join, 0)]
+        only("end", run, plan)
+        plan = [(from_layer_inner, 3), (widen, 0), (mids, 0, 0), (fetch_inner, 2, 2)]
+        plan += [(fetch_inner, 1, b) for b in range(3)] + [(fetch, 2, 0), (fetch, 2, 1)]
+        plan += [(widen, 1), (mids, 1, 0), (mids, 1, 1), (widen, 2), (mids, 2, 0), (mids, 2, 1)]
+        plan += [(relay, 0, 0)] + [(fetch_inner, 3, b) for b in range(3)] + [(widen, 3)]
+        plan += [(relay, 1, 0), (relay, 1, 1), (mids, 3, 0), (mids, 3, 1), (relay, 2, 0), (relay, 2, 1)]
+        plan += [(mids, 0, 1), (narrow, 1), (relay, 3, 0), (relay, 3, 1), (join, 1), (narrow, 2)]
+        plan += [(relay, 0, 1), (join, 2), (narrow, 3), (join, 3), (narrow, 0), (join, 0)]
+        only("inner", run, plan)
+    else:
+        plan = [(from_layer, d) for d in range(1, n_z)]
+        for d in range(n_z):
+            plan += [(fetch, d, b) for b in range(n_tp - 1)] if d else []
+            plan += [(widen, d), (mids, d, 0), (mids, d, 1)]
+        for d in range(n_z):
+            plan += [(relay, d, 0), (relay, d, 1), (narrow, d), (join, d)]
+        run(plan)
 
     result = hidden_v[...] + sh_s[n_tp - 1].astype(F32)
     for b in range(n_tp - 1):
@@ -324,12 +434,29 @@
     result = result + acc_v[0] + pr_r[0].astype(F32)
     for d in range(1, n_z):
         with jax.named_scope(f"w_zr{d}"):
-            arrived(zr_r.at[d], zr_recv.at[d])
-        result = result + zr_r[d].astype(F32)
+            arrived(zr_r.at[layers[d]], zr_recv.at[layers[d]])
+        result = result + zr_r[layers[d]].astype(F32)
     out[...] = result.T.astype(BF16)
     with jax.named_scope("w_send"):
-        for copy in pending:
+        for copy, *_ in pending:
             copy.wait_send()
+
+        @pl.when(sp < n_sp - 1)
+        def _():
+            for copy in halo:
+                copy.wait_send()
+
+        def sent(sems):
+            for sem, size in sems:
+                like = own if size == (pos, feats) else mid_all.at[0, 0, pl.ds(0, size[0])]
+                pltpu.make_async_remote_copy(
+                    src_ref=like, dst_ref=like, send_sem=sem[0].at[sem[1:]],
+                    recv_sem=sem[0].at[sem[1:]], device_id=partner, device_id_type=MESH,
+                ).wait_send()
+
+        for where, sems in turns.items():
+            if sems:
+                only(where, sent, list(sems))
 
 
 def local(n_sp, n_tp, *args):
@@ -349,6 +476,16 @@
     anywhere = pl.BlockSpec(memory_space=pl.ANY)
     dma = pltpu.SemaphoreType.DMA
     scratch = [
+        pltpu.VMEM((feats, pos), BF16),
+        pltpu.VMEM((chans, pos), BF16),
+        pltpu.VMEM((chans, pos), BF16),
+        pltpu.VMEM((chans, pos), BF16),
+        pltpu.VMEM((1, pos), jnp.int32),
+        pltpu.VMEM(conv_taps.shape, F32),
+        pltpu.VMEM((1, chans), F32),
+        pltpu.VMEM((1, feats), F32),
+        pltpu.VMEM((routes.shape[1], pos), jnp.int32),
+        pltpu.VMEM((routes.shape[1], pos), F32),
         pltpu.VMEM((chans, width), BF16),
         pltpu.VMEM((width, hid), BF16),
         pltpu.VMEM((width, hid), BF16),
@@ -374,15 +511,15 @@
         pltpu.VMEM((n_z, pos, feats), BF16),
         pltpu.VMEM((n_z, pos, feats), BF16),
         pltpu.VMEM((n_z, pos, feats), BF16),
-        dma((7,)),
+        dma((10,)), dma((7,)),
         dma((2,)), dma((2,)),
-        dma((n_tp,)), dma((n_tp,)),
+        dma((2, n_tp)), dma((2, n_tp)),
         dma((n_tp,)), dma((n_tp,)),
         dma((n_sp,)), dma((n_sp,)),
         dma((n_sp, n_tp)),
-        dma((n_z, n_tp)), dma((n_z,)), dma((n_z,)), dma((n_tp,)), dma((n_z, n_tp)),
+        dma((n_z, n_tp)), dma((n_z,)), dma((4, n_z)), dma((n_tp,)), dma((n_z, n_tp)),
         dma((n_tp,)), dma((n_tp,)),
-        dma((n_z, n_tp)), dma((n_z, n_tp)),
+        dma((n_z, 2, n_tp)), dma((n_z, 2, n_tp)),
         dma((n_z, 2)), dma((n_z, 2)),
         dma((n_z,)), dma((n_z,)),
         dma((n_z,)), dma((n_z,)),
@@ -390,7 +527,7 @@
     return pl.pallas_call(
         functools.partial(kernel, n_sp, n_tp, cap),
         out_shape=jax.ShapeDtypeStruct((feats, pos), BF16),
-        in_specs=[vmem] * 7 + [anywhere] + [vmem] * 3 + [anywhere] * 6,
+        in_specs=[anywhere] * 17,
         out_specs=vmem,
         scratch_shapes=scratch,
         compiler_params=pltpu.CompilerParams(

time: 81.3 us -> 71.8 us (0.88)
  Pallas kernels: 79.2 us -> 70 us
    pallas_call x1, Pallas kernels: 79.2 us -> 70 us  [local(): pl.pallas_call(functools.partial(kernel, n_sp, n_tp, cap), out_shape=jax....]
where the time goes in v2:
time: 71.8 us; the launch traced here: 71.6 us
  Pallas kernels  70 us (97%)
  local copies, waits for them, and re-layouts  1.57 us (2%)
    pallas_call x1, Pallas kernels, local(): pl.pallas_call(functools.partial(kernel, n_sp, n_tp, cap), out_shape=jax....  70 us
    unnamed x1, local copies, waits for them, and re-layouts  1.57 us

profile of v2, /device:TPU:0, one launch (start us, length us, event | category | flops | bytes accessed | tf_op | source)
XLA Modules:
  0.0 71.6 jit_solution(12907597388559118722)
XLA Ops:
  0.0 70.0 %shard_map.163 = bf16[512,128]{1,0:T(8,128)(2,1)} custom-call(bf16[512,128]{1,0:T(8,128)(2,1)} %stream_h.1, bf16[256,128]{1,0:T(8,128)(2,1)} %values_h.1, bf16[256,128]{1,0:T(8,128)(2,1)} %in_h.1, bf16[256,128]{1,0:T(8,128)(2,1)} %out_h.1, s32[1,128]{1,0:T(1,128)} %bitcast.9, f32[3,256]{1,0:T(4,128)} %taps_h.1, f32[1,256]{1,0:T(1,128)} %bitcast.8, ...), custom_call_target="tpu_custom_call" | custom-call | tf_op jit(solution)/shard_map/pallas_call | solution.py:527
  70.0 1.6 %copy.19 = bf16[512,128]{1,0:T(8,128)(2,1)} copy(bf16[512,128]{1,0:T(8,128)(2,1)} %shard_map.163) | data formatting | bytes 262144

commit v3 on v2

--- a/solution.py
+++ b/solution.py
@@ -48,10 +48,10 @@
     stream, values_in, in_gate, out_gate, documents, conv_taps, head_gain,
     norm_gain, routes, route_weight, mix_w, gate_w, up_w, sgate_w, sup_w, sdown_w, down_w,
     tail_s, prev_r, prev_docs, mix_s, mix_r, hidden_v, x_all, ss_s, ss_r, meta_r,
-    sh_s, sh_r, mid_all, acc_v, pr_s, pr_r, zr_s, zr_r,
+    sh_s, sh_r, mid_all, part_v, acc_v, pr_s, pr_r, zr_s, zr_r,
     small_sem, load_sem, halo_send, halo_recv, mix_send, mix_recv, ss_send, ss_recv,
-    meta_send, meta_recv, x_recv, xs_tp, xs_z, xs_r, xs_n, xs_p, sh_send, sh_recv,
-    mid_send, mid_recv, fwd_send, fwd_recv, pr_send, pr_recv, zr_send, zr_recv,
+    meta_send, meta_recv, xm_recv, xo_recv, xs_send, xb_send, sh_send, sh_recv,
+    mid_send, mid_recv, fwd_recv, pr_recv, zr_recv,
 ):
     sp = lax.axis_index("sp")
     tp = lax.axis_index("tp")
@@ -67,33 +67,65 @@
     square = n_tp == 4 and n_z == 4
     near = peers[:2] if square else peers
     layers = [flipped(z, d) for d in range(n_z)]
-    pending = []
     inner = lax.div(z + 1, 2) == 1
     if square:
         layers[2:] = [jnp.where(inner, layers[3], layers[2]), jnp.where(inner, layers[2], layers[3])]
-    turns = {"inner": [], "end": []}
+    branch = [""]
+    counts = {}
 
     def only(where, stage, *args):
         @pl.when(inner if where == "inner" else jnp.logical_not(inner))
         def _():
-            kept = len(pending)
+            branch[0] = where
             stage(*args)
-            turns[where].extend((sem, size) for _, sem, size in pending[kept:])
-            del pending[kept:]
-
-    def onward(block, rsem, slot, d):
-        def relay_on():
-            send(block, block, (xs_r, slot, d), rsem, {"sp": layers[2 if d < 2 else 1] * CORES + core})
-        return relay_on
-
-    def send(src, dst, ssem, rsem, device):
-        sem = ssem[0].at[ssem[1:]] if isinstance(ssem, tuple) else ssem
-        copy = pltpu.make_async_remote_copy(
+            branch[0] = ""
+
+    def far_own():
+        for d in (2, 3):
+            send(x_all.at[sp, tp], x_all.at[sp, tp], "x", xm_recv.at[z, tp],
+                 {"sp": layers[d] * CORES + core})
+
+    def onward(d, slice_of):
+        block = x_all.at[layers[d] * CORES + core, slice_of]
+        send(block, block, "x", xm_recv.at[layers[d], slice_of],
+             {"sp": layers[2 if d < 2 else 1] * CORES + core})
+
+    def across(d, slice_of):
+        block = x_all.at[layers[d] * CORES + core, slice_of]
+        send(block, block, "x", xo_recv.at[layers[d]], partner)
+
+    def send(src, dst, kind, rsem, device):
+        if isinstance(kind, str):
+            key = (branch[0], kind)
+            at = counts.get(key, 0)
+            counts[key] = at + 1
+            if kind == "mid":
+                sem = mid_send.at[at // (2 * n_tp)]
+            else:
+                sem = (xb_send if branch[0] else xs_send).at[at // n_tp]
+        else:
+            sem = kind
+        pltpu.make_async_remote_copy(
             src_ref=src, dst_ref=dst, send_sem=sem, recv_sem=rsem,
             device_id=device, device_id_type=MESH,
-        )
-        copy.start()
-        pending.append((copy, ssem, src.shape))
+        ).start()
+
+    def sent(like, sem):
+        pltpu.make_async_remote_copy(
+            src_ref=like, dst_ref=like, send_sem=sem, recv_sem=sem,
+            device_id=partner, device_id_type=MESH,
+        ).wait_send()
+
+    def all_sent(where):
+        for kind, size in (("x", n_tp), ("mid", 2 * n_tp)):
+            left, at = counts.get((where, kind), 0), 0
+            while left > 0:
+                now = min(left, size)
+                if kind == "x":
+                    sent(x_all.at[0, pl.ds(0, now)], (xb_send if where else xs_send).at[at])
+                else:
+                    sent(mid_all.at[0, pl.ds(0, now // 2)], mid_send.at[at])
+                left, at = left - now, at + 1
 
     def arrived(dst, rsem):
         pltpu.make_async_remote_copy(
@@ -159,11 +191,10 @@
             cols = pl.ds(pl.multiple_of(peer * feats, feats), feats)
             mix_s[b, rows[0]:rows[1]] = dot(heads_t[rows[0]:rows[1]], mix_w[:, cols]).astype(BF16)
 
-    def send_mix(rows, stage):
+    def send_mix(rows):
         part = pl.ds(rows[0], rows[1] - rows[0])
         for b, peer in enumerate(peers):
-            send(mix_s.at[b, part], mix_r.at[b, part], mix_send.at[stage, b],
-                 mix_recv.at[stage, b], {"tp": peer})
+            send(mix_s.at[b, part], mix_r.at[b, part], mix_send, mix_recv.at[b], {"tp": peer})
 
     heads_t = heads_of(None, jnp.full((1, pos), -1, jnp.int32))
     loads[0].wait()
@@ -188,7 +219,7 @@
         for copy in halo:
             copy.start()
 
-    send_mix((EDGE, pos), 0)
+    send_mix((EDGE, pos))
 
     @pl.when(sp == 0)
     def _():
@@ -204,7 +235,7 @@
 
     heads_t = heads_of(prev_r[...].T, prev_docs[...])
     mix((0, EDGE), heads_t)
-    send_mix((0, EDGE), 1)
+    send_mix((0, EDGE))
 
     named = routes[...]
     weights = route_weight[...]
@@ -218,8 +249,7 @@
     hidden = stream_t + mix_s[n_tp - 1].astype(F32)
     for b in range(n_tp - 1):
         with jax.named_scope(f"w_mix{b}"):
-            arrived(mix_r.at[b, pl.ds(EDGE, pos - EDGE)], mix_recv.at[0, b])
-            arrived(mix_r.at[b, pl.ds(0, EDGE)], mix_recv.at[1, b])
+            arrived(mix_r.at[b], mix_recv.at[b])
         hidden = hidden + mix_r[b].astype(F32)
     hidden_v[...] = hidden
     x_all[sp, tp] = (hidden * norm_gain[...]).astype(BF16)
@@ -227,49 +257,51 @@
     row = jnp.broadcast_to(squares, (pos, pos)).T[:SUB]
     ss_s[...] = row
     for b, peer in enumerate(peers):
-        send(ss_s, ss_r.at[b], ss_send.at[b], ss_recv.at[b], {"tp": peer})
+        send(ss_s, ss_r.at[b], ss_send, ss_recv, {"tp": peer})
     own = x_all.at[sp, tp]
     for b, peer in enumerate(peers):
-        send(own, own, (xs_tp, 0, b), x_recv.at[sp, tp], {"tp": peer})
+        send(own, own, "x", xm_recv.at[z, tp], {"tp": peer})
     for d in ([1] if square else range(1, n_z)):
-        send(own, own, (xs_z, d), x_recv.at[sp, tp], {"sp": layers[d] * CORES + core})
+        send(own, own, "x", xm_recv.at[z, tp], {"sp": layers[d] * CORES + core})
     if square:
-        only("inner", onward(own, x_recv.at[sp, tp], 0, 0))
-    send(own, own, (xs_p, 0, 0), x_recv.at[sp, tp], partner)
-
+        only("inner", far_own)
+    across(0, tp)
+
+    with jax.named_scope("w_ss"):
+        arrived(ss_r, ss_recv)
     for b in range(n_tp - 1):
-        with jax.named_scope(f"w_ss{b}"):
-            arrived(ss_r.at[b], ss_recv.at[b])
         row = row + ss_r[b]
     scale = lax.rsqrt(row[:1] / width + epsilon)
     meta_r[sp] = jnp.where(at_row == meta_rows - 1, scale, table)
     for d in range(1, n_sp):
-        send(meta_r.at[sp], meta_r.at[sp], meta_send.at[d], meta_recv.at[sp],
+        send(meta_r.at[sp], meta_r.at[sp], meta_send, meta_recv.at[sp],
              {"sp": lax.rem(sp + d, n_sp)})
 
-    def to_partner(slot, b, group):
-        block = x_all.at[group, peers[b]]
-        with jax.named_scope(f"w_x{slot}_{b}"):
-            arrived(block, x_recv.at[group, peers[b]])
-        send(block, block, (xs_p, slot, b + 1), x_recv.at[group, peers[b]], partner)
+    def fetch(d, b):
+        with jax.named_scope(f"w_x{d}_{b}"):
+            arrived(x_all.at[layers[d] * CORES + core, peers[b]], xm_recv.at[layers[d], peers[b]])
+        across(d, peers[b])
+
+    def fetch_inner(d, b):
+        fetch(d, b)
+        onward(d, peers[b])
 
     def from_layer(d):
-        group = layers[d] * CORES + core
-        block = x_all.at[group, tp]
+        block = x_all.at[layers[d] * CORES + core, tp]
         with jax.named_scope(f"w_layer{d}"):
-            arrived(block, x_recv.at[group, tp])
+            arrived(block, xm_recv.at[layers[d], tp])
         for b, peer in enumerate([] if square and d != 2 else near):
-            send(block, block, (xs_tp, d, b), x_recv.at[group, tp], {"tp": peer})
-        send(block, block, (xs_p, d, 0), x_recv.at[group, tp], partner)
+            send(block, block, "x", xm_recv.at[layers[d], tp], {"tp": peer})
+        across(d, tp)
+
+    def from_layer_inner(d):
+        from_layer(d)
+        if d != 2:
+            onward(d, tp)
 
     def closer(b):
         block = x_all.at[sp, peers[b]]
-        send(block, block, (xs_n, b), x_recv.at[sp, peers[b]], {"sp": layers[1] * CORES + core})
-
-    def from_layer_inner(d):
-        group = layers[d] * CORES + core
-        from_layer(d)
-        onward(x_all.at[group, tp], x_recv.at[group, tp], 0, d)()
+        send(block, block, "x", xm_recv.at[z, peers[b]], {"sp": layers[1] * CORES + core})
 
     if square:
         only("inner", from_layer_inner, 1)
@@ -287,20 +319,39 @@
 
     gate, upward = shared_part(tp)
     for b in range(n_tp - 1):
-        to_partner(0, b, sp)
-        block = x_all.at[sp, peers[b]]
+        fetch(0, b)
         if square:
             closer(b)
         if square and b == 2:
-            only("inner", onward(block, x_recv.at[sp, peers[2]], 3, 0))
+            only("inner", onward, 0, peers[2])
         more = shared_part(peers[b])
         gate, upward = gate + more[0], upward + more[1]
     shared_mid = (silu(gate * scale_own) * (upward * scale_own)).astype(BF16)
-    for b, peer in enumerate(peers + [tp]):
+    half = pos // 2
+
+    def shared_to(b, part, slot, i):
+        part = pl.ds(part * half, half)
+        rsem = sh_recv.at[1 + i] if slot == 2 else sh_recv.at[0]
+        send(sh_s.at[b, part], sh_r.at[slot, part], sh_send, rsem, {"tp": peers[i]})
+
+    for b in ([2, 0, 1, 3] if square else range(n_tp)):
+        peer = (peers + [tp])[b]
         cols = pl.ds(pl.multiple_of(peer * feats, feats), feats)
         sh_s[b] = dot(shared_mid, sdown_w[:, cols]).astype(BF16)
-        if b < n_tp - 1:
-            send(sh_s.at[b], sh_r.at[b], sh_send.at[b], sh_recv.at[b], {"tp": peer})
+        if square and b == 2:
+            shared_to(2, 0, 2, 0)
+            shared_to(2, 1, 2, 1)
+        elif square and b < 2:
+            shared_to(b, b, 0, b)
+        elif b < n_tp - 1:
+            send(sh_s.at[b], sh_r.at[b], sh_send, sh_recv.at[0], {"tp": peer})
+
+    def shared_on(i):
+        rows = slice(i * half, (i + 1) * half)
+        with jax.named_scope(f"w_shared{i}"):
+            arrived(sh_r.at[2, pl.ds(i * half, half)], sh_recv.at[1 + i])
+        sh_s[1 - i, rows] = (sh_s[1 - i, rows].astype(F32) + sh_r[2, rows].astype(F32)).astype(BF16)
+        shared_to(1 - i, i, 1, 1 - i)
 
     with jax.named_scope("w_load2"):
         for i in (4, 5, 6):
@@ -321,61 +372,62 @@
         count = dot(jnp.broadcast_to(mask, (2 * SUB, pos)).astype(BF16), earlier)[:1]
         return weight, jnp.where(weight > 0.0, count, -1.0)
 
-    def fetch(d, b):
-        to_partner(d, b, groups_of(d)[0])
-
-    def fetch_inner(d, b):
-        group = groups_of(d)[0]
-        to_partner(d, b, group)
-        block = x_all.at[group, peers[b]]
-        onward(block, x_recv.at[group, peers[b]], b + 1, d)()
-
-    def widen(d):
-        mine, other = groups_of(d)
-        with jax.named_scope(f"w_other{d}"):
-            if d > 0:
-                arrived(meta_r.at[mine], meta_recv.at[mine])
-            arrived(meta_r.at[other], meta_recv.at[other])
-            for b in range(n_tp):
-                arrived(x_all.at[other, b], x_recv.at[other, b])
-        gate = jnp.zeros((CORES * pos, hid), F32)
-        upward = jnp.zeros((CORES * pos, hid), F32)
+    def widen(d, which=(0, 1)):
+        groups = [groups_of(d)[i] for i in which]
+        for i, group in zip(which, groups):
+            with jax.named_scope(f"w_group{d}_{i}"):
+                if d > 0 or i > 0:
+                    arrived(meta_r.at[group], meta_recv.at[group])
+                if i > 0:
+                    arrived(x_all.at[group], xo_recv.at[layers[d]])
+        rows = len(groups) * pos
+        gate = jnp.zeros((rows, hid), F32)
+        upward = jnp.zeros((rows, hid), F32)
         for b in range(n_tp):
-            block = jnp.concatenate([x_all[mine, b], x_all[other, b]], axis=0)
+            block = jnp.concatenate([x_all[group, b] for group in groups], axis=0)
             gate = gate + dot(block, gate_w[b * feats:(b + 1) * feats, :])
             upward = upward + dot(block, up_w[b * feats:(b + 1) * feats, :])
         scales = jnp.concatenate([
-            column_of(meta_r[group, meta_rows - 1:, :], pos)[:, :1] for group in (mine, other)
+            column_of(meta_r[group, meta_rows - 1:, :], pos)[:, :1] for group in groups
         ], axis=0)
         middle = (silu(gate * scales) * (upward * scales)).astype(BF16)
-        for i, group in enumerate((mine, other)):
+        for at, (i, group) in enumerate(zip(which, groups)):
             slot = slots_of(group)[1]
             pick = jnp.where(rank_row == slot, 1.0, 0.0).astype(BF16)
             mid_all[d, tp, i * cap:(i + 1) * cap, :] = dot(
-                pick, middle[i * pos:(i + 1) * pos]
+                pick, middle[at * pos:(at + 1) * pos]
             ).astype(BF16)
 
     def mids(d, i):
         block = mid_all.at[d, tp, pl.ds(i * cap, cap)]
         for b, peer in enumerate(near):
-            send(block, block, (mid_send, d, i, b), mid_recv.at[d, i, tp], {"tp": peer})
+            send(block, block, "mid", mid_recv.at[d, i, b], {"tp": peer})
 
     def relay(d, i):
         for b, peer in enumerate(near):
             part = mid_all.at[d, peer, pl.ds(i * cap, cap)]
             with jax.named_scope(f"w_mid{d}_{i}_{b}"):
-                arrived(part, mid_recv.at[d, i, peer])
+                arrived(part, mid_recv.at[d, i, b])
             if square and b == i:
-                send(part, part, (fwd_send, d, i), fwd_recv.at[d, i], {"tp": near[1 - b]})
+                send(part, part, "mid", fwd_recv.at[d], {"tp": near[1 - b]})
+
+    def down(d, peer):
+        rows = pl.ds(pl.multiple_of(peer * hid, hid), hid)
+        return dot(mid_all[d, peer], down_w[rows, :])
+
+    def gather(d):
+        total = down(d, tp)
+        for peer in near:
+            total = total + down(d, peer)
+        part_v[d] = total
 
     def narrow(d):
         if square:
-            for b in range(2):
-                with jax.named_scope(f"w_fwd{d}_{b}"):
-                    arrived(mid_all.at[d, peers[2], pl.ds(b * cap, cap)], fwd_recv.at[d, b])
-        total = jnp.zeros((CORES * cap, feats), F32)
-        for b in range(n_tp):
-            total = total + dot(mid_all[d, b], down_w[b * hid:(b + 1) * hid, :])
+            with jax.named_scope(f"w_fwd{d}"):
+                arrived(mid_all.at[d, peers[2]], fwd_recv.at[d])
+        total = part_v[d]
+        if square:
+            total = total + down(d, peers[2])
         total = total.astype(BF16)
         terms = []
         for i, group in enumerate(groups_of(d)):
@@ -385,15 +437,34 @@
             terms.append(term * column_of(weight, pos)[:, :1])
         acc_v[d] = terms[0]
         pr_s[d] = terms[1].astype(BF16)
-        send(pr_s.at[d], pr_r.at[d], (pr_send, d), pr_recv.at[d], partner)
+        send(pr_s.at[d], pr_r.at[d], "x", pr_recv.at[d], partner)
 
     def join(d):
         with jax.named_scope(f"w_pr{d}"):
             arrived(pr_r.at[d], pr_recv.at[d])
-        if d > 0:
-            zr_s[d] = (acc_v[d] + pr_r[d].astype(F32)).astype(BF16)
-            send(zr_s.at[d], zr_r.at[z], (zr_send, d), zr_recv.at[z],
-                 {"sp": layers[d] * CORES + core})
+        if d == 0:
+            return
+        total = acc_v[d] + pr_r[d].astype(F32)
+        zr_s[d] = total.astype(BF16)
+        slot = {"inner": (0, 1, 1), "end": (0, 2, 2)}[branch[0]][d - 1] if square else d - 1
+        send(zr_s.at[d], zr_r.at[slot], "x", zr_recv, {"sp": layers[d] * CORES + core})
+
+    def finish():
+        result = hidden_v[...] + sh_s[n_tp - 1].astype(F32)
+        blocks = 2 if square else n_tp - 1
+        with jax.named_scope("w_sh"):
+            arrived(sh_r.at[pl.ds(0, blocks)], sh_recv.at[0])
+        for b in range(blocks):
+            result = result + sh_r[b].astype(F32)
+        result = result + acc_v[0] + pr_r[0].astype(F32)
+        if n_z > 1:
+            with jax.named_scope("w_zr"):
+                arrived(zr_r, zr_recv)
+        for d in range(1, n_z):
+            result = result + zr_r[d - 1].astype(F32)
+        out[...] = result.T.astype(BF16)
+        with jax.named_scope("w_sent"):
+            all_sent(branch[0])
 
     def run(plan):
         for stage, *where in plan:
@@ -401,21 +472,24 @@
 
     if square:
         plan = [(from_layer, 1), (widen, 0), (mids, 0, 0), (from_layer, 2), (mids, 0, 1)]
-        plan += [(fetch, 1, b) for b in range(3)] + [(widen, 1), (mids, 1, 0), (mids, 1, 1)]
-        plan += [(relay, 0, 0), (relay, 0, 1), (from_layer, 3)]
+        plan += [(fetch, 1, b) for b in range(3)] + [(shared_on, 0), (shared_on, 1)]
+        plan += [(widen, 1), (mids, 1, 0), (mids, 1, 1), (relay, 0, 0), (relay, 0, 1), (from_layer, 3)]
         plan += [(fetch, 2, b) for b in range(3)] + [(widen, 2), (mids, 2, 0), (mids, 2, 1)]
-        plan += [(relay, 1, 0), (relay, 1, 1), (relay, 2, 0)]
-        plan += [(fetch, 3, b) for b in range(3)] + [(widen, 3), (mids, 3, 0), (mids, 3, 1)]
-        plan += [(relay, 2, 1), (narrow, 1), (relay, 3, 0), (join, 1), (relay, 3, 1)]
-        plan += [(narrow, 2), (join, 2), (narrow, 0), (narrow, 3), (join, 3), (join, 0)]
+        plan += [(relay, 1, 0), (relay, 1, 1)] + [(fetch, 3, b) for b in range(3)]
+        plan += [(widen, 3, (0,)), (mids, 3, 0), (widen, 3, (1,)), (mids, 3, 1)]
+        plan += [(relay, 2, 0), (relay, 2, 1), (gather, 1), (narrow, 1), (gather, 2), (relay, 3, 0), (join, 1)]
+        plan += [(gather, 0), (relay, 3, 1), (narrow, 2), (gather, 3), (join, 2), (narrow, 3)]
+        plan += [(narrow, 0), (join, 3), (join, 0), (finish,)]
         only("end", run, plan)
         plan = [(from_layer_inner, 3), (widen, 0), (mids, 0, 0), (fetch_inner, 2, 2)]
         plan += [(fetch_inner, 1, b) for b in range(3)] + [(fetch, 2, 0), (fetch, 2, 1)]
-        plan += [(widen, 1), (mids, 1, 0), (mids, 1, 1), (widen, 2), (mids, 2, 0), (mids, 2, 1)]
-        plan += [(relay, 0, 0)] + [(fetch_inner, 3, b) for b in range(3)] + [(widen, 3)]
-        plan += [(relay, 1, 0), (relay, 1, 1), (mids, 3, 0), (mids, 3, 1), (relay, 2, 0), (relay, 2, 1)]
-        plan += [(mids, 0, 1), (narrow, 1), (relay, 3, 0), (relay, 3, 1), (join, 1), (narrow, 2)]
-        plan += [(relay, 0, 1), (join, 2), (narrow, 3), (join, 3), (narrow, 0), (join, 0)]
+        plan += [(shared_on, 0), (shared_on, 1), (widen, 1), (mids, 1, 0)]
+        plan += [(widen, 2), (mids, 2, 0), (mids, 2, 1), (mids, 1, 1)]
+        plan += [(fetch_inner, 3, b) for b in range(3)] + [(widen, 3), (mids, 3, 0), (mids, 3, 1)]
+        plan += [(relay, 2, 0), (relay, 2, 1), (gather, 2), (relay, 3, 0), (relay, 3, 1)]
+        plan += [(relay, 1, 0), (relay, 1, 1), (mids, 0, 1), (relay, 0, 0), (narrow, 2), (gather, 3)]
+        plan += [(narrow, 3), (join, 2), (gather, 1), (join, 3), (narrow, 1), (join, 1)]
+        plan += [(relay, 0, 1), (gather, 0), (narrow, 0), (join, 0), (finish,)]
         only("inner", run, plan)
     else:
         plan = [(from_layer, d) for d in range(1, n_z)]
@@ -423,40 +497,20 @@
             plan += [(fetch, d, b) for b in range(n_tp - 1)] if d else []
             plan += [(widen, d), (mids, d, 0), (mids, d, 1)]
         for d in range(n_z):
-            plan += [(relay, d, 0), (relay, d, 1), (narrow, d), (join, d)]
-        run(plan)
-
-    result = hidden_v[...] + sh_s[n_tp - 1].astype(F32)
-    for b in range(n_tp - 1):
-        with jax.named_scope(f"w_sh{b}"):
-            arrived(sh_r.at[b], sh_recv.at[b])
-        result = result + sh_r[b].astype(F32)
-    result = result + acc_v[0] + pr_r[0].astype(F32)
-    for d in range(1, n_z):
-        with jax.named_scope(f"w_zr{d}"):
-            arrived(zr_r.at[layers[d]], zr_recv.at[layers[d]])
-        result = result + zr_r[layers[d]].astype(F32)
-    out[...] = result.T.astype(BF16)
+            plan += [(relay, d, 0), (relay, d, 1), (gather, d), (narrow, d), (join, d)]
+        run(plan + [(finish,)])
+
     with jax.named_scope("w_send"):
-        for copy, *_ in pending:
-            copy.wait_send()
+        all_sent("")
+        sent(mix_s.at[pl.ds(0, n_tp - 1)], mix_send)
+        sent(ss_r, ss_send)
+        sent(meta_r.at[pl.ds(0, n_sp - 1)], meta_send)
+        sent(sh_s.at[pl.ds(0, 3 if square else n_tp - 1)], sh_send)
 
         @pl.when(sp < n_sp - 1)
         def _():
             for copy in halo:
                 copy.wait_send()
-
-        def sent(sems):
-            for sem, size in sems:
-                like = own if size == (pos, feats) else mid_all.at[0, 0, pl.ds(0, size[0])]
-                pltpu.make_async_remote_copy(
-                    src_ref=like, dst_ref=like, send_sem=sem[0].at[sem[1:]],
-                    recv_sem=sem[0].at[sem[1:]], device_id=partner, device_id_type=MESH,
-                ).wait_send()
-
-        for where, sems in turns.items():
-            if sems:
-                only(where, sent, list(sems))
 
 
 def local(n_sp, n_tp, *args):
@@ -472,6 +526,9 @@
     experts = n_sp * expert_gate.shape[0]
     bound = 3 * pos * routes.shape[1] // (2 * experts)
     cap = -(-bound // (2 * SUB)) * 2 * SUB
+    square = n_tp == 4 and n_z == 4
+    near = 2 if square else n_tp - 1
+    sends = (11, 34) if square else (n_tp * (2 * n_z + 1) * 2, 1)
     vmem = pl.BlockSpec(memory_space=pltpu.VMEM)
     anywhere = pl.BlockSpec(memory_space=pl.ANY)
     dma = pltpu.SemaphoreType.DMA
@@ -501,37 +558,36 @@
         pltpu.VMEM((pos, feats), F32),
         pltpu.VMEM((n_sp, n_tp, pos, feats), BF16),
         pltpu.VMEM((SUB, pos), F32),
-        pltpu.VMEM((n_tp, SUB, pos), F32),
+        pltpu.VMEM((n_tp - 1, SUB, pos), F32),
         pltpu.VMEM((n_sp, meta_rows, pos), F32),
         pltpu.VMEM((n_tp, pos, feats), BF16),
         pltpu.VMEM((n_tp, pos, feats), BF16),
         pltpu.VMEM((n_z, n_tp, CORES * cap, hid), BF16),
+        pltpu.VMEM((n_z, CORES * cap, feats), F32),
         pltpu.VMEM((n_z, pos, feats), F32),
         pltpu.VMEM((n_z, pos, feats), BF16),
         pltpu.VMEM((n_z, pos, feats), BF16),
         pltpu.VMEM((n_z, pos, feats), BF16),
-        pltpu.VMEM((n_z, pos, feats), BF16),
+        pltpu.VMEM((max(n_z - 1, 1), pos, feats), BF16),
         dma((10,)), dma((7,)),
         dma((2,)), dma((2,)),
-        dma((2, n_tp)), dma((2, n_tp)),
-        dma((n_tp,)), dma((n_tp,)),
-        dma((n_sp,)), dma((n_sp,)),
-        dma((n_sp, n_tp)),
-        dma((n_z, n_tp)), dma((n_z,)), dma((4, n_z)), dma((n_tp,)), dma((n_z, n_tp)),
-        dma((n_tp,)), dma((n_tp,)),
-        dma((n_z, 2, n_tp)), dma((n_z, 2, n_tp)),
-        dma((n_z, 2)), dma((n_z, 2)),
-        dma((n_z,)), dma((n_z,)),
-        dma((n_z,)), dma((n_z,)),
+        dma, dma((n_tp - 1,)),
+        dma, dma,
+        dma, dma((n_sp,)),
+        dma((n_z, n_tp)), dma((n_z,)), dma((-(-sends[0] // n_tp),)), dma((-(-sends[1] // n_tp),)),
+        dma, dma((3,)),
+        dma((n_z,)), dma((n_z, 2, near)), dma((n_z,)),
+        dma((n_z,)), dma,
     ]
     return pl.pallas_call(
         functools.partial(kernel, n_sp, n_tp, cap),
-        out_shape=jax.ShapeDtypeStruct((feats, pos), BF16),
+        out_shape=pltpu.VMEM((feats, pos), BF16),
         in_specs=[anywhere] * 17,
         out_specs=vmem,
         scratch_shapes=scratch,
         compiler_params=pltpu.CompilerParams(
-            collective_id=0, has_side_effects=True, vmem_limit_bytes=64 * 1024 * 1024 - 65536
+            collective_id=0, has_side_effects=True,
+            vmem_limit_bytes=64 * 1024 * 1024 - 65536 - 2 * feats * pos,
         ),
     )(
         stream, values_in, in_gate, out_gate, documents.reshape(1, pos), conv_taps,

time: 71.8 us -> 66.2 us (0.922)
  Pallas kernels: 70 us -> 65.4 us
  local copies, waits for them, and re-layouts: 1.57 us -> 0.66 us
    pallas_call x1, Pallas kernels: 70 us -> 65.4 us  [local(): pl.pallas_call(functools.partial(kernel, n_sp, n_tp, cap), out_shape=pltp...]
    unnamed x1, local copies, waits for them, and re-layouts: 1.57 us -> 0.66 us
where the time goes in v3:
time: 66.2 us; the launch traced here: 66 us
  Pallas kernels  65.4 us (99%)
    pallas_call x1, Pallas kernels, local(): pl.pallas_call(functools.partial(kernel, n_sp, n_tp, cap), out_shape=pltp...  65.4 us

profile of v3, /device:TPU:0, one launch (start us, length us, event | category | flops | bytes accessed | tf_op | source)
XLA Modules:
  0.0 66.0 jit_solution(7448193593022943013)
XLA Ops:
  0.0 65.4 %shard_map.163 = bf16[512,128]{1,0:T(8,128)(2,1)S(1)} custom-call(bf16[512,128]{1,0:T(8,128)(2,1)} %stream_h.1, bf16[256,128]{1,0:T(8,128)(2,1)} %values_h.1, bf16[256,128]{1,0:T(8,128)(2,1)} %in_h.1, bf16[256,128]{1,0:T(8,128)(2,1)} %out_h.1, s32[1,128]{1,0:T(1,128)} %bitcast.9, f32[3,256]{1,0:T(4,128)} %taps_h.1, f32[1,256]{1,0:T(1,128)} %bitcast.8, ...), custom_call_target="tpu_custom_call" | custom-call | tf_op jit(solution)/shard_map/pallas_call | solution.py:582
  65.4 0.7 copy.19

commit v4 on v3

--- a/solution.py
+++ b/solution.py
@@ -48,7 +48,7 @@
     stream, values_in, in_gate, out_gate, documents, conv_taps, head_gain,
     norm_gain, routes, route_weight, mix_w, gate_w, up_w, sgate_w, sup_w, sdown_w, down_w,
     tail_s, prev_r, prev_docs, mix_s, mix_r, hidden_v, x_all, ss_s, ss_r, meta_r,
-    sh_s, sh_r, mid_all, part_v, acc_v, pr_s, pr_r, zr_s, zr_r,
+    sh_s, sh_r, mid_all, part_v, place_v, column_v, early_v, acc_v, pr_s, pr_r, zr_s, zr_r,
     small_sem, load_sem, halo_send, halo_recv, mix_send, mix_recv, ss_send, ss_recv,
     meta_send, meta_recv, xm_recv, xo_recv, xs_send, xb_send, sh_send, sh_recv,
     mid_send, mid_recv, fwd_recv, pr_recv, zr_recv,
@@ -191,6 +191,19 @@
             cols = pl.ds(pl.multiple_of(peer * feats, feats), feats)
             mix_s[b, rows[0]:rows[1]] = dot(heads_t[rows[0]:rows[1]], mix_w[:, cols]).astype(BF16)
 
+    def mix_part(b, rows, slot, i, rsem):
+        part = pl.ds(rows[0], rows[1] - rows[0])
+        send(mix_s.at[b, part], mix_r.at[slot, part], mix_send, mix_recv.at[rsem], {"tp": peers[i]})
+
+    parts = ((EDGE, pos // 2), (pos // 2, pos))
+
+    def mix_on(i):
+        rows = slice(*parts[i])
+        with jax.named_scope(f"w_mixd{i}"):
+            arrived(mix_r.at[2, pl.ds(parts[i][0], parts[i][1] - parts[i][0])], mix_recv.at[2 + i])
+        mix_s[1 - i, rows] = (mix_s[1 - i, rows].astype(F32) + mix_r[2, rows].astype(F32)).astype(BF16)
+        mix_part(1 - i, parts[i], 1, 1 - i, 1)
+
     def send_mix(rows):
         part = pl.ds(rows[0], rows[1] - rows[0])
         for b, peer in enumerate(peers):
@@ -219,7 +232,13 @@
         for copy in halo:
             copy.start()
 
-    send_mix((EDGE, pos))
+    if square:
+        for i in range(2):
+            mix_part(2, parts[i], 2, i, 2 + i)
+        for i in range(2):
+            mix_part(i, parts[i], 0, i, 0)
+    else:
+        send_mix((EDGE, pos))
 
     @pl.when(sp == 0)
     def _():
@@ -235,7 +254,13 @@
 
     heads_t = heads_of(prev_r[...].T, prev_docs[...])
     mix((0, EDGE), heads_t)
-    send_mix((0, EDGE))
+    if square:
+        for b in (2, 0, 1):
+            mix_part(b, (0, EDGE), b, b, 4)
+        mix_on(0)
+        mix_on(1)
+    else:
+        send_mix((0, EDGE))
 
     named = routes[...]
     weights = route_weight[...]
@@ -247,7 +272,15 @@
     stream_t = stream[...].astype(F32).T
 
     hidden = stream_t + mix_s[n_tp - 1].astype(F32)
-    for b in range(n_tp - 1):
+    if square:
+        with jax.named_scope("w_mix"):
+            arrived(mix_r.at[0, pl.ds(EDGE, pos - EDGE)], mix_recv.at[0])
+            arrived(mix_r.at[1, pl.ds(EDGE, pos - EDGE)], mix_recv.at[1])
+            arrived(mix_r.at[2, pl.ds(0, 3 * EDGE)], mix_recv.at[4])
+        hidden = hidden + mix_r[0].astype(F32) + mix_r[1].astype(F32)
+        edge = mix_r[2, :EDGE].astype(F32)
+        hidden = hidden + jnp.concatenate([edge, jnp.zeros((pos - EDGE, feats), F32)], axis=0)
+    for b in range(0 if square else n_tp - 1):
         with jax.named_scope(f"w_mix{b}"):
             arrived(mix_r.at[b], mix_recv.at[b])
         hidden = hidden + mix_r[b].astype(F32)
@@ -372,7 +405,17 @@
         count = dot(jnp.broadcast_to(mask, (2 * SUB, pos)).astype(BF16), earlier)[:1]
         return weight, jnp.where(weight > 0.0, count, -1.0)
 
-    def widen(d, which=(0, 1)):
+    def expert_part(group, peer):
+        rows = pl.ds(pl.multiple_of(peer * feats, feats), feats)
+        block = x_all[group, peer]
+        return dot(block, gate_w[rows, :]), dot(block, up_w[rows, :])
+
+    def begin(d):
+        parts = [expert_part(groups_of(d)[0], peer) for peer in (tp, *near)]
+        for i in range(2):
+            early_v[i] = sum([part[i] for part in parts[1:]], parts[0][i])
+
+    def widen(d, which=(0, 1), ready=False):
         groups = [groups_of(d)[i] for i in which]
         for i, group in zip(which, groups):
             with jax.named_scope(f"w_group{d}_{i}"):
@@ -383,7 +426,10 @@
         rows = len(groups) * pos
         gate = jnp.zeros((rows, hid), F32)
         upward = jnp.zeros((rows, hid), F32)
-        for b in range(n_tp):
+        if ready:
+            more = expert_part(groups[0], peers[2])
+            gate, upward = early_v[0] + more[0], early_v[1] + more[1]
+        for b in range(0 if ready else n_tp):
             block = jnp.concatenate([x_all[group, b] for group in groups], axis=0)
             gate = gate + dot(block, gate_w[b * feats:(b + 1) * feats, :])
             upward = upward + dot(block, up_w[b * feats:(b + 1) * feats, :])
@@ -420,6 +466,10 @@
         for peer in near:
             total = total + down(d, peer)
         part_v[d] = total
+        for i, group in enumerate(groups_of(d)):
+            weight, slot = slots_of(group)
+            place_v[d, i] = jnp.where(rank_lane == column_of(slot, cap), 1.0, 0.0).astype(BF16)
+            column_v[d, i] = column_of(weight, pos)
 
     def narrow(d):
         if square:
@@ -429,15 +479,13 @@
         if square:
             total = total + down(d, peers[2])
         total = total.astype(BF16)
-        terms = []
-        for i, group in enumerate(groups_of(d)):
-            weight, slot = slots_of(group)
-            place = jnp.where(rank_lane == column_of(slot, cap), 1.0, 0.0).astype(BF16)
-            term = dot(place, total[i * cap:(i + 1) * cap])
-            terms.append(term * column_of(weight, pos)[:, :1])
-        acc_v[d] = terms[0]
-        pr_s[d] = terms[1].astype(BF16)
-        send(pr_s.at[d], pr_r.at[d], "x", pr_recv.at[d], partner)
+        for i in (1, 0):
+            term = dot(place_v[d, i], total[i * cap:(i + 1) * cap]) * column_v[d, i][:, :1]
+            if i == 1:
+                pr_s[d] = term.astype(BF16)
+                send(pr_s.at[d], pr_r.at[d], "x", pr_recv.at[d], partner)
+            else:
+                acc_v[d] = term
 
     def join(d):
         with jax.named_scope(f"w_pr{d}"):
@@ -475,8 +523,8 @@
         plan += [(fetch, 1, b) for b in range(3)] + [(shared_on, 0), (shared_on, 1)]
         plan += [(widen, 1), (mids, 1, 0), (mids, 1, 1), (relay, 0, 0), (relay, 0, 1), (from_layer, 3)]
         plan += [(fetch, 2, b) for b in range(3)] + [(widen, 2), (mids, 2, 0), (mids, 2, 1)]
-        plan += [(relay, 1, 0), (relay, 1, 1)] + [(fetch, 3, b) for b in range(3)]
-        plan += [(widen, 3, (0,)), (mids, 3, 0), (widen, 3, (1,)), (mids, 3, 1)]
+        plan += [(relay, 1, 0), (relay, 1, 1), (fetch, 3, 0), (fetch, 3, 1), (begin, 3), (fetch, 3, 2)]
+        plan += [(widen, 3, (0,), True), (mids, 3, 0), (widen, 3, (1,)), (mids, 3, 1)]
         plan += [(relay, 2, 0), (relay, 2, 1), (gather, 1), (narrow, 1), (gather, 2), (relay, 3, 0), (join, 1)]
         plan += [(gather, 0), (relay, 3, 1), (narrow, 2), (gather, 3), (join, 2), (narrow, 3)]
         plan += [(narrow, 0), (join, 3), (join, 0), (finish,)]
@@ -564,6 +612,9 @@
         pltpu.VMEM((n_tp, pos, feats), BF16),
         pltpu.VMEM((n_z, n_tp, CORES * cap, hid), BF16),
         pltpu.VMEM((n_z, CORES * cap, feats), F32),
+        pltpu.VMEM((n_z, CORES, pos, cap), BF16),
+        pltpu.VMEM((n_z, CORES, pos, pos), F32),
+        pltpu.VMEM((2, pos, hid), F32),
         pltpu.VMEM((n_z, pos, feats), F32),
         pltpu.VMEM((n_z, pos, feats), BF16),
         pltpu.VMEM((n_z, pos, feats), BF16),
@@ -571,7 +622,7 @@
         pltpu.VMEM((max(n_z - 1, 1), pos, feats), BF16),
         dma((10,)), dma((7,)),
         dma((2,)), dma((2,)),
-        dma, dma((n_tp - 1,)),
+        dma, dma((max(n_tp - 1, 5),)),
         dma, dma,
         dma, dma((n_sp,)),
         dma((n_z, n_tp)), dma((n_z,)), dma((-(-sends[0] // n_tp),)), dma((-(-sends[1] // n_tp),)),

time: 66.2 us -> 65.3 us (0.986)
  Pallas kernels: 65.4 us -> 64.5 us
    pallas_call x1, Pallas kernels: 65.4 us -> 64.5 us  [local(): pl.pallas_call(functools.partial(kernel, n_sp, n_tp, cap), out_shape=pltp...]
where the time goes in v4:
time: 65.3 us; the launch traced here: 65.1 us
  Pallas kernels  64.5 us (99%)
  local copies, waits for them, and re-layouts  0.66 us (1%)
    pallas_call x1, Pallas kernels, local(): pl.pallas_call(functools.partial(kernel, n_sp, n_tp, cap), out_shape=pltp...  64.5 us

profile of v4, /device:TPU:0, one launch (start us, length us, event | category | flops | bytes accessed | tf_op | source)
XLA Modules:
  0.0 65.1 jit_solution(5427416747453397216)
XLA Ops:
  0.0 64.5 %shard_map.163 = bf16[512,128]{1,0:T(8,128)(2,1)S(1)} custom-call(bf16[512,128]{1,0:T(8,128)(2,1)} %stream_h.1, bf16[256,128]{1,0:T(8,128)(2,1)} %values_h.1, bf16[256,128]{1,0:T(8,128)(2,1)} %in_h.1, bf16[256,128]{1,0:T(8,128)(2,1)} %out_h.1, s32[1,128]{1,0:T(1,128)} %bitcast.9, f32[3,256]{1,0:T(4,128)} %taps_h.1, f32[1,256]{1,0:T(1,128)} %bitcast.8, ...), custom_call_target="tpu_custom_call" | custom-call | tf_op jit(solution)/shard_map/pallas_call | solution.py:633
  64.5 0.7 %copy.19 = bf16[512,128]{1,0:T(8,128)(2,1)} copy(bf16[512,128]{1,0:T(8,128)(2,1)S(1)} %shard_map.163) | data formatting | bytes 262144

commit v5 on v4

--- a/solution.py
+++ b/solution.py
@@ -40,7 +40,7 @@
 
 
 def kernel(
-    n_sp, n_tp, cap,
+    n_sp, n_tp, cap, n_mid,
     stream_h, values_h, in_h, out_h, documents_h, taps_h, head_h, mix_weight,
     norm_h, routes_h, route_weight_h, expert_gate, expert_up, expert_down,
     shared_gate, shared_up, shared_down,
@@ -49,9 +49,9 @@
     norm_gain, routes, route_weight, mix_w, gate_w, up_w, sgate_w, sup_w, sdown_w, down_w,
     tail_s, prev_r, prev_docs, mix_s, mix_r, hidden_v, x_all, ss_s, ss_r, meta_r,
     sh_s, sh_r, mid_all, part_v, place_v, column_v, early_v, acc_v, pr_s, pr_r, zr_s, zr_r,
-    small_sem, load_sem, halo_send, halo_recv, mix_send, mix_recv, ss_send, ss_recv,
-    meta_send, meta_recv, xm_recv, xo_recv, xs_send, xb_send, sh_send, sh_recv,
-    mid_send, mid_recv, fwd_recv, pr_recv, zr_recv,
+    pool, load_sem, halo_send, halo_recv, mix_recv, ss_recv,
+    meta_recv, xm_recv, xo_recv, xb_send, sh_recv,
+    mid_recv, fwd_recv, pr_recv, zr_recv,
 ):
     sp = lax.axis_index("sp")
     tp = lax.axis_index("tp")
@@ -70,6 +70,7 @@
     inner = lax.div(z + 1, 2) == 1
     if square:
         layers[2:] = [jnp.where(inner, layers[3], layers[2]), jnp.where(inner, layers[2], layers[3])]
+    mix_send, ss_send, meta_send, sh_send = (pool.at[i] for i in range(4))
     branch = [""]
     counts = {}
 
@@ -81,7 +82,7 @@
             branch[0] = ""
 
     def far_own():
-        for d in (2, 3):
+        for d in (3, 2):
             send(x_all.at[sp, tp], x_all.at[sp, tp], "x", xm_recv.at[z, tp],
                  {"sp": layers[d] * CORES + core})
 
@@ -100,9 +101,9 @@
             at = counts.get(key, 0)
             counts[key] = at + 1
             if kind == "mid":
-                sem = mid_send.at[at // (2 * n_tp)]
+                sem = pool.at[4 + at // (2 * n_tp)]
             else:
-                sem = (xb_send if branch[0] else xs_send).at[at // n_tp]
+                sem = xb_send.at[at // n_tp] if branch[0] else pool.at[4 + n_mid + at // n_tp]
         else:
             sem = kind
         pltpu.make_async_remote_copy(
@@ -122,9 +123,10 @@
             while left > 0:
                 now = min(left, size)
                 if kind == "x":
-                    sent(x_all.at[0, pl.ds(0, now)], (xb_send if where else xs_send).at[at])
+                    sem = xb_send.at[at] if where else pool.at[4 + n_mid + at]
+                    sent(x_all.at[0, pl.ds(0, now)], sem)
                 else:
-                    sent(mid_all.at[0, pl.ds(0, now // 2)], mid_send.at[at])
+                    sent(mid_all.at[0, pl.ds(0, now // 2)], pool.at[4 + at])
                 left, at = left - now, at + 1
 
     def arrived(dst, rsem):
@@ -142,7 +144,7 @@
         ])
     ]
     smalls = [
-        pltpu.make_async_copy(src, dst, small_sem.at[i])
+        pltpu.make_async_copy(src, dst, pool.at[i])
         for i, (src, dst) in enumerate([
             (values_h, values_in), (in_h, in_gate), (documents_h, documents), (out_h, out_gate),
             (taps_h, conv_taps), (head_h, head_gain), (routes_h, routes),
@@ -151,12 +153,12 @@
     ]
 
     barrier = pltpu.get_barrier_semaphore()
-    for peer in peers:
-        pl.semaphore_signal(barrier, inc=1, device_id={"tp": peer}, device_id_type=MESH)
     for d in range(1, n_sp):
         pl.semaphore_signal(
             barrier, inc=1, device_id={"sp": lax.rem(sp + d, n_sp)}, device_id_type=MESH
         )
+    for peer in peers:
+        pl.semaphore_signal(barrier, inc=1, device_id={"tp": peer}, device_id_type=MESH)
     for copy in smalls:
         copy.start()
     loads[0].start()
@@ -338,7 +340,6 @@
 
     if square:
         only("inner", from_layer_inner, 1)
-        only("inner", from_layer_inner, 2)
 
     with jax.named_scope("w_load"):
         for i in (1, 2, 3):
@@ -357,6 +358,7 @@
             closer(b)
         if square and b == 2:
             only("inner", onward, 0, peers[2])
+            only("end", from_layer, 2)
         more = shared_part(peers[b])
         gate, upward = gate + more[0], upward + more[1]
     shared_mid = (silu(gate * scale_own) * (upward * scale_own)).astype(BF16)
@@ -519,17 +521,17 @@
             stage(*where)
 
     if square:
-        plan = [(from_layer, 1), (widen, 0), (mids, 0, 0), (from_layer, 2), (mids, 0, 1)]
+        plan = [(from_layer, 1), (widen, 0), (mids, 0, 0), (mids, 0, 1)]
         plan += [(fetch, 1, b) for b in range(3)] + [(shared_on, 0), (shared_on, 1)]
         plan += [(widen, 1), (mids, 1, 0), (mids, 1, 1), (relay, 0, 0), (relay, 0, 1), (from_layer, 3)]
         plan += [(fetch, 2, b) for b in range(3)] + [(widen, 2), (mids, 2, 0), (mids, 2, 1)]
         plan += [(relay, 1, 0), (relay, 1, 1), (fetch, 3, 0), (fetch, 3, 1), (begin, 3), (fetch, 3, 2)]
         plan += [(widen, 3, (0,), True), (mids, 3, 0), (widen, 3, (1,)), (mids, 3, 1)]
         plan += [(relay, 2, 0), (relay, 2, 1), (gather, 1), (narrow, 1), (gather, 2), (relay, 3, 0), (join, 1)]
-        plan += [(gather, 0), (relay, 3, 1), (narrow, 2), (gather, 3), (join, 2), (narrow, 3)]
+        plan += [(gather, 0), (relay, 3, 1), (gather, 3), (narrow, 2), (join, 2), (narrow, 3)]
         plan += [(narrow, 0), (join, 3), (join, 0), (finish,)]
         only("end", run, plan)
-        plan = [(from_layer_inner, 3), (widen, 0), (mids, 0, 0), (fetch_inner, 2, 2)]
+        plan = [(from_layer_inner, 2), (from_layer_inner, 3), (widen, 0), (mids, 0, 0), (fetch_inner, 2, 2)]
         plan += [(fetch_inner, 1, b) for b in range(3)] + [(fetch, 2, 0), (fetch, 2, 1)]
         plan += [(shared_on, 0), (shared_on, 1), (widen, 1), (mids, 1, 0)]
         plan += [(widen, 2), (mids, 2, 0), (mids, 2, 1), (mids, 1, 1)]
@@ -577,6 +579,7 @@
     square = n_tp == 4 and n_z == 4
     near = 2 if square else n_tp - 1
     sends = (11, 34) if square else (n_tp * (2 * n_z + 1) * 2, 1)
+    n_mid = 3 if square else n_z
     vmem = pl.BlockSpec(memory_space=pltpu.VMEM)
     anywhere = pl.BlockSpec(memory_space=pl.ANY)
     dma = pltpu.SemaphoreType.DMA
@@ -620,18 +623,14 @@
         pltpu.VMEM((n_z, pos, feats), BF16),
         pltpu.VMEM((n_z, pos, feats), BF16),
         pltpu.VMEM((max(n_z - 1, 1), pos, feats), BF16),
-        dma((10,)), dma((7,)),
+        dma((max(10, 4 + n_mid - (-sends[0] // n_tp)),)), dma((7,)),
         dma((2,)), dma((2,)),
-        dma, dma((max(n_tp - 1, 5),)),
-        dma, dma,
-        dma, dma((n_sp,)),
-        dma((n_z, n_tp)), dma((n_z,)), dma((-(-sends[0] // n_tp),)), dma((-(-sends[1] // n_tp),)),
-        dma, dma((3,)),
-        dma((n_z,)), dma((n_z, 2, near)), dma((n_z,)),
-        dma((n_z,)), dma,
+        dma((max(n_tp - 1, 5),)), dma,
+        dma((n_sp,)), dma((n_z, n_tp)), dma((n_z,)), dma((-(-sends[1] // n_tp),)), dma((3,)),
+        dma((n_z, 2, near)), dma((n_z,)), dma((n_z,)), dma,
     ]
     return pl.pallas_call(
-        functools.partial(kernel, n_sp, n_tp, cap),
+        functools.partial(kernel, n_sp, n_tp, cap, n_mid),
         out_shape=pltpu.VMEM((feats, pos), BF16),
         in_specs=[anywhere] * 17,
         out_specs=vmem,

time: 65.3 us -> 64.3 us (0.985)
  Pallas kernels: 64.5 us -> 63.5 us
    pallas_call x1, Pallas kernels: 64.5 us -> 63.5 us  [local(): pl.pallas_call(functools.partial(kernel, n_sp, n_tp, cap, n_mid), out_sha...]
where the time goes in v5:
time: 64.3 us; the launch traced here: 64.2 us
  Pallas kernels  63.5 us (99%)
  local copies, waits for them, and re-layouts  0.66 us (1%)
    pallas_call x1, Pallas kernels, local(): pl.pallas_call(functools.partial(kernel, n_sp, n_tp, cap, n_mid), out_sha...  63.5 us

profile of v5, /device:TPU:0, one launch (start us, length us, event | category | flops | bytes accessed | tf_op | source)
XLA Modules:
  0.0 64.2 jit_solution(1763125041392577720)
XLA Ops:
  0.0 63.5 %shard_map.163 = bf16[512,128]{1,0:T(8,128)(2,1)S(1)} custom-call(bf16[512,128]{1,0:T(8,128)(2,1)} %stream_h.1, bf16[256,128]{1,0:T(8,128)(2,1)} %values_h.1, bf16[256,128]{1,0:T(8,128)(2,1)} %in_h.1, bf16[256,128]{1,0:T(8,128)(2,1)} %out_h.1, s32[1,128]{1,0:T(1,128)} %bitcast.9, f32[3,256]{1,0:T(4,128)} %taps_h.1, f32[1,256]{1,0:T(1,128)} %bitcast.8, ...), custom_call_target="tpu_custom_call" | custom-call | tf_op jit(solution)/shard_map/pallas_call | solution.py:632
  63.5 0.7 %copy.19 = bf16[512,128]{1,0:T(8,128)(2,1)} copy(bf16[512,128]{1,0:T(8,128)(2,1)S(1)} %shard_map.163) | data formatting | bytes 262144

commit v6 on v5

--- a/solution.py
+++ b/solution.py
@@ -50,7 +50,7 @@
     tail_s, prev_r, prev_docs, mix_s, mix_r, hidden_v, x_all, ss_s, ss_r, meta_r,
     sh_s, sh_r, mid_all, part_v, place_v, column_v, early_v, acc_v, pr_s, pr_r, zr_s, zr_r,
     pool, load_sem, halo_send, halo_recv, mix_recv, ss_recv,
-    meta_recv, xm_recv, xo_recv, xb_send, sh_recv,
+    meta_recv, xm_recv, xo_recv, sh_recv,
     mid_recv, fwd_recv, pr_recv, zr_recv,
 ):
     sp = lax.axis_index("sp")
@@ -103,7 +103,7 @@
             if kind == "mid":
                 sem = pool.at[4 + at // (2 * n_tp)]
             else:
-                sem = xb_send.at[at // n_tp] if branch[0] else pool.at[4 + n_mid + at // n_tp]
+                sem = load_sem.at[at // n_tp] if branch[0] else pool.at[4 + n_mid + at // n_tp]
         else:
             sem = kind
         pltpu.make_async_remote_copy(
@@ -123,7 +123,7 @@
             while left > 0:
                 now = min(left, size)
                 if kind == "x":
-                    sem = xb_send.at[at] if where else pool.at[4 + n_mid + at]
+                    sem = load_sem.at[at] if where else pool.at[4 + n_mid + at]
                     sent(x_all.at[0, pl.ds(0, now)], sem)
                 else:
                     sent(mid_all.at[0, pl.ds(0, now // 2)], pool.at[4 + at])
@@ -273,6 +273,8 @@
         table = table + jnp.where(at_row == named[k:k + 1, :], weights[k:k + 1, :], 0.0)
     stream_t = stream[...].astype(F32).T
 
+    for load in loads[1:]:
+        load.wait()
     hidden = stream_t + mix_s[n_tp - 1].astype(F32)
     if square:
         with jax.named_scope("w_mix"):
@@ -341,9 +343,6 @@
     if square:
         only("inner", from_layer_inner, 1)
 
-    with jax.named_scope("w_load"):
-        for i in (1, 2, 3):
-            loads[i].wait()
     scale_own = column_of(scale, pos)[:, :1]
 
     def shared_part(peer):
@@ -388,9 +387,6 @@
         sh_s[1 - i, rows] = (sh_s[1 - i, rows].astype(F32) + sh_r[2, rows].astype(F32)).astype(BF16)
         shared_to(1 - i, i, 1, 1 - i)
 
-    with jax.named_scope("w_load2"):
-        for i in (4, 5, 6):
-            loads[i].wait()
 
     at_a = lax.broadcasted_iota(jnp.int32, (pos, pos), 0)
     at_b = lax.broadcasted_iota(jnp.int32, (pos, pos), 1)
@@ -523,13 +519,13 @@
     if square:
         plan = [(from_layer, 1), (widen, 0), (mids, 0, 0), (mids, 0, 1)]
         plan += [(fetch, 1, b) for b in range(3)] + [(shared_on, 0), (shared_on, 1)]
-        plan += [(widen, 1), (mids, 1, 0), (mids, 1, 1), (relay, 0, 0), (relay, 0, 1), (from_layer, 3)]
+        plan += [(widen, 1), (mids, 1, 0), (mids, 1, 1), (from_layer, 3)]
         plan += [(fetch, 2, b) for b in range(3)] + [(widen, 2), (mids, 2, 0), (mids, 2, 1)]
         plan += [(relay, 1, 0), (relay, 1, 1), (fetch, 3, 0), (fetch, 3, 1), (begin, 3), (fetch, 3, 2)]
         plan += [(widen, 3, (0,), True), (mids, 3, 0), (widen, 3, (1,)), (mids, 3, 1)]
-        plan += [(relay, 2, 0), (relay, 2, 1), (gather, 1), (narrow, 1), (gather, 2), (relay, 3, 0), (join, 1)]
-        plan += [(gather, 0), (relay, 3, 1), (gather, 3), (narrow, 2), (join, 2), (narrow, 3)]
-        plan += [(narrow, 0), (join, 3), (join, 0), (finish,)]
+        plan += [(relay, 2, 0), (relay, 2, 1), (gather, 1), (narrow, 1), (gather, 2), (relay, 3, 0)]
+        plan += [(join, 1), (relay, 3, 1), (relay, 0, 0), (relay, 0, 1), (gather, 3), (narrow, 2)]
+        plan += [(join, 2), (narrow, 3), (gather, 0), (join, 3), (narrow, 0), (join, 0), (finish,)]
         only("end", run, plan)
         plan = [(from_layer_inner, 2), (from_layer_inner, 3), (widen, 0), (mids, 0, 0), (fetch_inner, 2, 2)]
         plan += [(fetch_inner, 1, b) for b in range(3)] + [(fetch, 2, 0), (fetch, 2, 1)]
@@ -623,10 +619,10 @@
         pltpu.VMEM((n_z, pos, feats), BF16),
         pltpu.VMEM((n_z, pos, feats), BF16),
         pltpu.VMEM((max(n_z - 1, 1), pos, feats), BF16),
-        dma((max(10, 4 + n_mid - (-sends[0] // n_tp)),)), dma((7,)),
+        dma((max(10, 4 + n_mid - (-sends[0] // n_tp)),)), dma((max(7, -(-sends[1] // n_tp)),)),
         dma((2,)), dma((2,)),
         dma((max(n_tp - 1, 5),)), dma,
-        dma((n_sp,)), dma((n_z, n_tp)), dma((n_z,)), dma((-(-sends[1] // n_tp),)), dma((3,)),
+        dma((n_sp,)), dma((n_z, n_tp)), dma((n_z,)), dma((3,)),
         dma((n_z, 2, near)), dma((n_z,)), dma((n_z,)), dma,
     ]
     return pl.pallas_call(

time: 64.3 us -> 64.2 us (level)
  no operation moved by 1% of the time
where the time goes in v6:
time: 64.2 us; the launch traced here: 64.1 us
  Pallas kernels  63.4 us (99%)
  local copies, waits for them, and re-layouts  0.66 us (1%)
    pallas_call x1, Pallas kernels, local(): pl.pallas_call(functools.partial(kernel, n_sp, n_tp, cap, n_mid), out_sha...  63.4 us

profile of v6, /device:TPU:0, one launch (start us, length us, event | category | flops | bytes accessed | tf_op | source)
XLA Modules:
  0.0 64.1 jit_solution(13991143998941501257)
XLA Ops:
  0.0 63.4 %shard_map.163 = bf16[512,128]{1,0:T(8,128)(2,1)S(1)} custom-call(bf16[512,128]{1,0:T(8,128)(2,1)} %stream_h.1, bf16[256,128]{1,0:T(8,128)(2,1)} %values_h.1, bf16[256,128]{1,0:T(8,128)(2,1)} %in_h.1, bf16[256,128]{1,0:T(8,128)(2,1)} %out_h.1, s32[1,128]{1,0:T(1,128)} %bitcast.9, f32[3,256]{1,0:T(4,128)} %taps_h.1, f32[1,256]{1,0:T(1,128)} %bitcast.8, ...), custom_call_target="tpu_custom_call" | custom-call | tf_op jit(solution)/shard_map/pallas_call | solution.py:628
  63.4 0.7 %copy.19 = bf16[512,128]{1,0:T(8,128)(2,1)} copy(bf16[512,128]{1,0:T(8,128)(2,1)S(1)} %shard_map.163) | data formatting | bytes 262144
